TPU v7x, 32 devices: a whole 2x2x4 slice. The times are simulated.
32 devices in a mesh: ep: 8 (over z, x), tp: 4 (over y, core).
Axes of the slice: x: 2, y: 2, z: 4, core: 2. Of those that a mesh axis runs over, the one named last changes fastest.
Arguments:
- resid: bfloat16 [256, 2048], P('ep'), may hold values from -6 to 6
- norm_gain: bfloat16 [2048], replicated, may hold values from 0.099609375 to 1.8984375
- w_query: bfloat16 [2048, 1024], P(None, 'tp'), may hold values from -0.125 to 0.125
- w_key: bfloat16 [2048, 1024], P(None, 'tp'), may hold values from -0.125 to 0.125
- w_value: bfloat16 [2048, 1024], P(None, 'tp'), may hold values from -0.125 to 0.125
- w_gate: bfloat16 [2048, 1024], P(None, 'tp'), may hold values from -0.125 to 0.125
- head_gain: bfloat16 [1024], P('tp'), may hold values from 0.099609375 to 1.8984375
- w_output: bfloat16 [1024, 2048], P('tp'), may hold values from -0.1875 to 0.1875
- state: float32 [256, 8, 128, 128], P('ep', 'tp'), may hold values from -0.6 to 0.6
- positions: int32 [256], P('ep'), may hold values from 1024 to 8191
- ffn_gain: bfloat16 [2048], replicated, may hold values from 0.099609375 to 1.8984375
- w_mix: bfloat16 [2048], replicated, may hold values from -0.125 to 0.125
- dense_gate: bfloat16 [2048, 5632], P('tp', 'ep'), may hold values from -0.125 to 0.125
- dense_up: bfloat16 [2048, 5632], P('tp', 'ep'), may hold values from -0.125 to 0.125
- dense_down: bfloat16 [5632, 2048], P('ep', 'tp'), may hold values from -0.109375 to 0.109375
- routes: int32 [256, 2], P('ep'), may hold values from 0 to 7, all different within a row; in each aligned block of 32 rows (0 to 31, 32 to 63, ...) at most 16 rows name the same one
- route_weight: bfloat16 [256, 2], P('ep'), may hold values from 0.19921875 to 1
- expert_gate: bfloat16 [8, 2048, 4096], P('ep', None, 'tp'), may hold values from -0.125 to 0.125
- expert_up: bfloat16 [8, 2048, 4096], P('ep', None, 'tp'), may hold values from -0.125 to 0.125
- expert_down: bfloat16 [8, 4096, 2048], P('ep', 'tp'), may hold values from -0.09375 to 0.09375
Outputs:
- final: bfloat16 [256, 2048], P('ep', 'tp')
- new_state: float32 [256, 8, 128, 128], P('ep', 'tp')
Inputs may be any that keep to these rules, and one draw needn't show every extreme that they name: `routes`: each row names 2 different experts; in the rows of one index of ep no expert is named by more than 16 rows, a bound that some block reaches; every expert is named by some row.
All inputs are finite; a program needn't handle non-finite values.
Results may differ from a plain program's by a relative error of at most 0.018.
Values may be sent and summed in bfloat16 or wider, within the bound.
A program may use at most 64 MiB of HBM per device.

v0:
```python
import functools

import jax
import jax.numpy as jnp
from jax import lax
from jax.experimental import pallas as pl
from jax.experimental.pallas import tpu as pltpu
from jax.sharding import PartitionSpec as P

EPSILON = 1e-06
THETA = 10000.0


def rms_norm(inputs, scaling):
    square = jnp.mean(inputs * inputs, axis=-1, keepdims=True)
    return inputs * lax.rsqrt(square + EPSILON) * scaling.astype(jnp.float32)


def rotate(inputs, places):
    halfway = inputs.shape[-1] // 2
    inverse = THETA ** (-jnp.arange(halfway, dtype=jnp.float32) / halfway)
    angles = places.astype(jnp.float32)[:, None] * inverse[None, :]
    cosine = jnp.cos(angles)[:, None, :]
    sine_of = jnp.sin(angles)[:, None, :]
    former = inputs[..., :halfway]
    latter = inputs[..., halfway:]
    return jnp.concatenate(
        [former * cosine - latter * sine_of, former * sine_of + latter * cosine], axis=-1
    )


def retain(queries, keys_in, values_in, gating, memory, places, head_first, head_gain):
    seqs_here = queries.shape[0]
    heads_here = memory.shape[1]
    head_size = memory.shape[2]
    head_shape = (seqs_here, heads_here, head_size)
    query_rot = rotate(queries.astype(jnp.float32).reshape(head_shape), places)
    key_rot = rotate(keys_in.astype(jnp.float32).reshape(head_shape), places) * head_size ** (-0.5)
    value_heads = values_in.astype(jnp.float32).reshape(head_shape)
    head_index = head_first + jnp.arange(heads_here, dtype=jnp.float32)
    decays = 1.0 - jnp.exp2(-1.0 - 1.5 * head_index)
    within = jnp.sum(query_rot * key_rot, axis=-1, keepdims=True) * value_heads
    carried = (
        jnp.einsum("shd,shde->she", query_rot, memory, precision=lax.Precision.HIGHEST)
        * decays[None, :, None]
    )
    mixture = within + carried
    new_memory = (
        decays[None, :, None, None] * memory + key_rot[:, :, :, None] * value_heads[:, :, None, :]
    )
    centre = jnp.mean(mixture, axis=-1, keepdims=True)
    spread = jnp.mean(jnp.square(mixture - centre), axis=-1, keepdims=True)
    normed = ((mixture - centre) * lax.rsqrt(spread + EPSILON)).reshape(
        seqs_here, heads_here * head_size
    )
    normed = normed * head_gain.astype(jnp.float32)
    output = (jax.nn.silu(gating.astype(jnp.float32)) * normed).astype(jnp.bfloat16)
    return (output, new_memory)


def routing(routes, route_weight, capacity, slots, experts_all):
    seq_dev, top_count = routes.shape
    flat_ids = routes.reshape(-1)
    expert_ids = jnp.arange(experts_all, dtype=jnp.int32)
    onehot = (flat_ids[:, None] == expert_ids[None, :]).astype(jnp.int32)
    ranks = jnp.sum((jnp.cumsum(onehot, axis=0) - 1) * onehot, axis=1)
    slot_ids = (flat_ids * slots + ranks).reshape(seq_dev, top_count)
    slot_range = jnp.arange(experts_all * slots, dtype=jnp.int32)
    hits = slot_ids[:, :, None] == slot_range[None, None, :]
    combine = jnp.sum(
        jnp.where(hits, route_weight.astype(jnp.float32)[:, :, None], 0.0), axis=1
    ).astype(jnp.bfloat16)
    dispatch = jnp.any(slot_range[:, None, None] == slot_ids[None, :, :], axis=2)
    dispatch = dispatch.astype(jnp.bfloat16).reshape(experts_all, slots, seq_dev)
    return dispatch, combine


def tail_kernel(
    tp_count,
    ep_count,
    slots,
    part_ref,
    resid_ref,
    scale_ref,
    dispatch_ref,
    combine_ref,
    dense_gate,
    dense_up,
    dense_down,
    expert_gate,
    expert_up,
    expert_down,
    out_ref,
    wg,
    wu,
    wd,
    eg,
    eu,
    ed,
    att_rx,
    middle,
    stat_tx,
    stat_rx,
    rows,
    hot,
    tokens,
    gu_tx,
    gu_rx,
    gu_pair,
    gu_far,
    hidden,
    eh,
    er_tx,
    er_rx,
    er_pair,
    er_far,
    do_tx,
    do_rx,
    mo_tx,
    mo_rx,
    load_sem,
    send_sem,
    recv_sem,
):
    me_t = lax.axis_index("tp")
    me_e = lax.axis_index("ep")
    seq_dev, model_width = resid_ref.shape
    width = model_width // tp_count
    block = hidden.shape[0] // tp_count
    f32 = jnp.float32
    bf16 = jnp.bfloat16

    loads = [
        pltpu.make_async_copy(source, target, load_sem.at[index])
        for index, (source, target) in enumerate(
            (
                (dense_gate, wg),
                (dense_up, wu),
                (expert_gate.at[0], eg),
                (expert_up.at[0], eu),
                (expert_down.at[0], ed),
                (dense_down, wd),
            )
        )
    ]
    for load in loads:
        load.start()

    def peer_t(step):
        return lax.rem(me_t + step, tp_count)

    def peer_e(step):
        return lax.rem(me_e + step, ep_count)

    barrier = pltpu.get_barrier_semaphore()
    for step in range(1, tp_count):
        pl.semaphore_signal(
            barrier,
            inc=1,
            device_id=(me_e, peer_t(step)),
            device_id_type=pl.DeviceIdType.MESH,
        )
    for step in range(1, ep_count):
        pl.semaphore_signal(
            barrier,
            inc=1,
            device_id=(peer_e(step), me_t),
            device_id_type=pl.DeviceIdType.MESH,
        )
    pl.semaphore_wait(barrier, tp_count - 1 + ep_count - 1)

    used = [0]
    started = []

    def send(source, target, device):
        index = used[0]
        used[0] = index + 1
        copy = pltpu.make_async_remote_copy(
            src_ref=source,
            dst_ref=target,
            send_sem=send_sem.at[index],
            recv_sem=recv_sem.at[index],
            device_id=device,
            device_id_type=pl.DeviceIdType.MESH,
        )
        copy.start()
        started.append(copy)
        return copy

    def span(index, size):
        return pl.ds(pl.multiple_of(index * size, size), size)

    def dot(left, right):
        return jnp.dot(left, right, preferred_element_type=f32)

    def arrive(copies):
        for copy in copies:
            copy.wait_recv()

    half = tp_count // 2
    sibling = me_t + 1 - 2 * lax.rem(me_t, 2)

    def across(index, step):
        return lax.rem(index + 2 * step, tp_count)

    def spread(at):
        return [
            send(at(me_t), at(me_t), (me_e, target))
            for target in [sibling] + [across(me_t, k) for k in range(1, half)]
        ]

    def pass_on(copies, at):
        waiting = [copies[0]]
        for k in range(1, half):
            copies[k].wait_recv()
            origin = across(me_t, half - k)
            waiting.append(send(at(origin), at(origin), (me_e, sibling)))
        return waiting

    tp_steps = range(1, tp_count)
    ep_steps = range(1, ep_count)
    own = span(me_t, width)

    att = [
        send(part_ref.at[:, span(peer_t(d), width)], att_rx.at[d - 1], (me_e, peer_t(d)))
        for d in tp_steps
    ]
    hots = [
        send(dispatch_ref.at[peer_e(d)], hot.at[me_e], (peer_e(d), me_t)) for d in ep_steps
    ]
    hot[me_e] = dispatch_ref[me_e]
    scales = scale_ref[:, own].astype(f32)
    gain = scales[0:1, :]
    mix = scales[1:2, :]
    arrive(att)
    total = part_ref[:, own].astype(f32)
    for d in tp_steps:
        total = total + att_rx[d - 1].astype(f32)
    mid = resid_ref[:, own].astype(f32) + total
    middle[...] = mid
    square = jnp.sum(mid * mid, axis=-1, keepdims=True)
    mixed = jnp.sum(mid * gain * mix, axis=-1, keepdims=True)
    lane = lax.broadcasted_iota(jnp.int32, stat_tx.shape, 1)
    stat = jnp.where(lane < 64, square, mixed)
    stat_tx[...] = stat
    stats = [send(stat_tx, stat_rx.at[d - 1], (me_e, peer_t(d))) for d in tp_steps]
    arrive(stats)
    for d in tp_steps:
        stat = stat + stat_rx[d - 1]
    inverse = lax.rsqrt(stat[:, 0:1] / model_width + EPSILON)
    mixing = jax.nn.sigmoid(inverse * stat[:, 64:65])
    rows[me_e] = (middle[...] * inverse * gain).astype(bf16)

    gathered = [send(rows.at[me_e], rows.at[me_e], (peer_e(d), me_t)) for d in ep_steps]
    arrive(hots)
    arrive(gathered)
    for s in range(ep_count):
        tokens[me_t, s * slots : (s + 1) * slots, :] = dot(hot[s], rows[s]).astype(bf16)
    toks = spread(lambda index: tokens.at[index])
    near = []
    all_rows = rows[...].reshape(ep_count * seq_dev, width)
    for which, weight in enumerate((wg, wu)):
        loads[which].wait()
        gu_tx[which] = lax.dot_general(
            all_rows, weight[...], (((1,), (1,)), ((), ())), preferred_element_type=f32
        ).astype(bf16)
        near.append(
            [
                send(
                    gu_tx.at[which, span(across(sibling, k), block), :],
                    gu_rx.at[which, k],
                    (me_e, sibling),
                )
                for k in range(half)
            ]
        )
    toks = pass_on(toks, lambda index: tokens.at[index])
    far = []
    for which in range(2):
        arrive(near[which])
        for k in range(1, half):
            target = across(me_t, k)
            gu_pair[which, k - 1] = (
                gu_tx[which, span(target, block), :].astype(f32) + gu_rx[which, k].astype(f32)
            ).astype(bf16)
            far.append(
                send(gu_pair.at[which, k - 1], gu_far.at[which, k - 1], (me_e, target))
            )
    loads[2].wait()
    loads[3].wait()
    arrive(toks)
    tile = min(256, eg.shape[1])

    def expert_tile(index, carry):
        columns = span(index, tile)
        gate = jnp.zeros((tokens.shape[1], tile), f32)
        up = jnp.zeros((tokens.shape[1], tile), f32)
        for c in range(tp_count):
            features = slice(c * width, (c + 1) * width)
            gate = gate + dot(tokens[c], eg[features, columns])
            up = up + dot(tokens[c], eu[features, columns])
        eh[:, columns] = (jax.nn.silu(gate) * up).astype(bf16)
        return carry

    lax.fori_loop(0, eg.shape[1] // tile, expert_tile, 0)

    arrive(far)
    gate = gu_tx[0, span(me_t, block), :].astype(f32) + gu_rx[0, 0].astype(f32)
    up = gu_tx[1, span(me_t, block), :].astype(f32) + gu_rx[1, 0].astype(f32)
    for k in range(1, half):
        gate = gate + gu_far[0, k - 1].astype(f32)
        up = up + gu_far[1, k - 1].astype(f32)
    hidden[span(me_t, block), :] = (jax.nn.silu(gate) * up).astype(bf16)
    hids = spread(lambda index: hidden.at[span(index, block), :])
    loads[4].wait()
    pairs = []
    for k in range(half):
        target = across(sibling, k)
        er_tx[k] = dot(eh[...], ed[:, span(target, width)]).astype(bf16)
        pairs.append(send(er_tx.at[k], er_rx.at[k], (me_e, sibling)))
    hids = pass_on(hids, lambda index: hidden.at[span(index, block), :])
    partials = []
    for k in range(1, half):
        target = across(me_t, k)
        summed = dot(eh[...], ed[:, span(target, width)])
        arrive(pairs[k : k + 1])
        er_pair[k - 1] = (summed + er_rx[k].astype(f32)).astype(bf16)
        partials.append(send(er_pair.at[k - 1], er_far.at[k - 1], (me_e, target)))
    loads[5].wait()
    arrive(hids)
    do_tx[...] = dot(hidden[...], wd[...]).astype(bf16)
    outs = [
        send(do_tx.at[span(peer_e(d), seq_dev), :], do_rx.at[d - 1], (peer_e(d), me_t))
        for d in ep_steps
    ]
    result = dot(eh[...], ed[:, own])
    arrive(pairs[:1])
    result = result + er_rx[0].astype(f32)
    arrive(partials)
    for k in range(1, half):
        result = result + er_far[k - 1].astype(f32)
    mo_tx[...] = result.astype(bf16)
    place = span(me_e, slots)
    backs = [
        send(mo_tx.at[span(peer_e(d), slots), :], mo_rx.at[place, :], (peer_e(d), me_t))
        for d in ep_steps
    ]
    mo_rx[place, :] = mo_tx[place, :]
    arrive(outs)
    dense = do_tx[span(me_e, seq_dev), :].astype(f32)
    for d in ep_steps:
        dense = dense + do_rx[d - 1].astype(f32)
    partly = middle[...] + mixing * dense
    arrive(backs)
    out_ref[...] = (partly + dot(combine_ref[...], mo_rx[...])).astype(bf16)
    for copy in started:
        copy.wait_send()


def tail(part, resid, scale, dispatch, combine, weights, tp_count, ep_count):
    seq_dev, model_width = resid.shape
    width = model_width // tp_count
    slots = dispatch.shape[1]
    batch = seq_dev * ep_count
    block = batch // tp_count
    dense_units = weights[0].shape[0]
    half = tp_count // 2
    expert_units = weights[3].shape[2]
    items = ep_count * slots
    bf16 = jnp.bfloat16
    peers_t = tp_count - 1
    peers_e = ep_count - 1
    copies = 7 * peers_t + 4 * peers_e
    vmem = pl.BlockSpec(memory_space=pltpu.VMEM)
    anywhere = pl.BlockSpec(memory_space=pltpu.HBM)
    return pl.pallas_call(
        functools.partial(tail_kernel, tp_count, ep_count, slots),
        out_shape=jax.ShapeDtypeStruct((seq_dev, width), bf16),
        in_specs=[vmem] * 5 + [anywhere] * 6,
        out_specs=vmem,
        scratch_shapes=[
            pltpu.VMEM(weights[0].shape, bf16),
            pltpu.VMEM(weights[1].shape, bf16),
            pltpu.VMEM(weights[2].shape, bf16),
            pltpu.VMEM(weights[3].shape[1:], bf16),
            pltpu.VMEM(weights[4].shape[1:], bf16),
            pltpu.VMEM(weights[5].shape[1:], bf16),
            pltpu.VMEM((peers_t, seq_dev, width), bf16),
            pltpu.VMEM((seq_dev, width), jnp.float32),
            pltpu.VMEM((seq_dev, 128), jnp.float32),
            pltpu.VMEM((peers_t, seq_dev, 128), jnp.float32),
            pltpu.VMEM((ep_count, seq_dev, width), bf16),
            pltpu.VMEM((ep_count, slots, seq_dev), bf16),
            pltpu.VMEM((tp_count, items, width), bf16),
            pltpu.VMEM((2, batch, dense_units), bf16),
            pltpu.VMEM((2, half, block, dense_units), bf16),
            pltpu.VMEM((2, half - 1, block, dense_units), bf16),
            pltpu.VMEM((2, half - 1, block, dense_units), bf16),
            pltpu.VMEM((batch, dense_units), bf16),
            pltpu.VMEM((items, expert_units), bf16),
            pltpu.VMEM((half, items, width), bf16),
            pltpu.VMEM((half, items, width), bf16),
            pltpu.VMEM((half - 1, items, width), bf16),
            pltpu.VMEM((half - 1, items, width), bf16),
            pltpu.VMEM((batch, width), bf16),
            pltpu.VMEM((peers_e, seq_dev, width), bf16),
            pltpu.VMEM((items, width), bf16),
            pltpu.VMEM((items, width), bf16),
            pltpu.SemaphoreType.DMA((6,)),
            pltpu.SemaphoreType.DMA((copies,)),
            pltpu.SemaphoreType.DMA((copies,)),
        ],
        compiler_params=pltpu.CompilerParams(
            collective_id=0, has_side_effects=True, vmem_limit_bytes=61 * 1024 * 1024
        ),
        name="tail",
    )(part, resid, scale, dispatch, combine, *weights)


def per_device(
    resid,
    norm_gain,
    w_query,
    w_key,
    w_value,
    w_gate,
    head_gain,
    w_output,
    state,
    positions,
    ffn_gain,
    w_mix,
    dense_gate,
    dense_up,
    dense_down,
    routes,
    route_weight,
    expert_gate,
    expert_up,
    expert_down,
):
    seq_dev = resid.shape[0]
    tp_count = lax.axis_size("tp")
    ep_count = lax.axis_size("ep")
    tp_index = lax.axis_index("tp")
    normed_in = rms_norm(resid.astype(jnp.float32), norm_gain).astype(jnp.bfloat16)

    def project(weight):
        return jnp.dot(normed_in, weight, preferred_element_type=jnp.float32).astype(jnp.bfloat16)

    heads_here = state.shape[1]
    head_first = (tp_index * heads_here).astype(jnp.float32)
    retained, new_state = retain(
        project(w_query),
        project(w_key),
        project(w_value),
        project(w_gate),
        state,
        positions,
        head_first,
        head_gain,
    )
    part = jnp.dot(retained, w_output, preferred_element_type=jnp.float32).astype(jnp.bfloat16)
    top_count = routes.shape[1]
    capacity = max(2, 2 * seq_dev * top_count // ep_count)
    slots = -(-capacity // 16) * 16
    dispatch, combine = routing(routes, route_weight, capacity, slots, ep_count)
    final = tail(
        part,
        resid,
        jnp.stack([ffn_gain, w_mix]),
        dispatch,
        combine,
        (dense_gate.T, dense_up.T, dense_down, expert_gate, expert_up, expert_down),
        tp_count,
        ep_count,
    )
    return (final, new_state)


def solution(mesh):
    in_specs = (
        P("ep", None),
        P(),
        P(None, "tp"),
        P(None, "tp"),
        P(None, "tp"),
        P(None, "tp"),
        P("tp"),
        P("tp", None),
        P("ep", "tp", None, None),
        P("ep"),
        P(),
        P(),
        P("tp", "ep"),
        P("tp", "ep"),
        P("ep", "tp"),
        P("ep", None),
        P("ep", None),
        P("ep", None, "tp"),
        P("ep", None, "tp"),
        P("ep", "tp", None),
    )
    out_specs = (P("ep", "tp"), P("ep", "tp", None, None))
    return jax.shard_map(
        per_device, mesh=mesh, in_specs=in_specs, out_specs=out_specs, check_vma=False
    )
```

profile of v0, /device:TPU:0, one launch (start us, length us, event | category | flops | bytes accessed | tf_op | source)
XLA Modules:
  0.0 72.7 jit_solution(13725866249245227797)
XLA Ops:
  0.6 0.0 copy-start
  0.7 0.7 %convert_element_type.65 = f32[32]{0:T(128)S(1)} convert(s32[32]{0:T(128)} %param.29) | non-fusion elementwise | flops 32 | bytes 256 | tf_op jit(solution)/shard_map/convert_element_type | solution.py:22
  1.4 1.0 %fusion.7 = f32[32]{0:T(128)S(1)} fusion(bf16[32,2048]{1,0:T(8,128)(2,1)} %resid_ref.1), kind=kLoop, calls=%fused_computation.15 | loop fusion | flops 196576 | bytes 131200 | tf_op jit(solution)/shard_map/reduce_sum | solution.py:15
  2.5 0.7 convert_element_type.69
  3.1 0.7 convert_element_type.75
  3.8 0.7 convert_element_type.60
  4.5 0.7 stack.9
  5.2 0.7 stack.10
  5.9 0.6 pad_maximum_fusion.1.scale_ref
  6.5 0.8 %copy.36 = s32[32,2]{1,0:T(8,128)S(1)} copy(s32[32,2]{0,1:T(2,128)} %param.35) | data formatting | bytes 512 | tf_op args[15]
  7.2 0.1 eq.42
  7.4 0.1 multiply_cosine_fusion
  7.5 0.1 fusion.12
  7.6 0.1 reduce_window_sum.11
  7.7 0.2 select_reduce_fusion.1
  7.9 0.1 reduce_sum.61
  8.0 0.1 copy.37
  8.0 0.7 multiply_add_fusion.3
  8.7 0.1 fusion.13
  8.8 0.7 select_reduce_fusion.combine_ref
  9.5 0.7 copy.38
  10.2 1.6 %fusion.5 = f32[32,256]{1,0:T(8,128)S(1)} fusion(bf16[2048,256]{1,0:T(8,128)(2,1)} %param.22, bf16[32,2048]{1,0:T(8,128)(2,1)} %resid_ref.1, f32[2048]{0:T(1024)S(1)} %convert_element_type.60, f32[32]{0:T(128)S(1)} %add_rsqrt_fusion.1), kind=kOutput, calls=%fused_computation.10 | convolution fusion | flops 33832960 | bytes 1220736 | tf_op jit(solution)/shard_map/dot_general | solution.py:449
  11.9 0.0 copy-start.1
  11.9 0.0 copy-start.2
  11.9 1.7 %fusion.4 = f32[32,256]{1,0:T(8,128)S(1)} fusion(bf16[2048,256]{1,0:T(8,128)(2,1)} %param.23, bf16[32,2048]{1,0:T(8,128)(2,1)} %resid_ref.1, f32[2048]{0:T(1024)S(1)} %convert_element_type.60, f32[32]{0:T(128)S(1)} %add_rsqrt_fusion.1), kind=kOutput, calls=%fused_computation.8 | convolution fusion | flops 33832960 | bytes 1220736 | tf_op jit(solution)/shard_map/dot_general | solution.py:449
  13.6 1.6 %fusion.3 = f32[32,256]{1,0:T(8,128)S(1)} fusion(bf16[2048,256]{1,0:T(8,128)(2,1)} %param.24, bf16[32,2048]{1,0:T(8,128)(2,1)} %resid_ref.1, f32[2048]{0:T(1024)S(1)} %convert_element_type.60, f32[32]{0:T(128)S(1)} %add_rsqrt_fusion.1), kind=kOutput, calls=%fused_computation.6 | convolution fusion | flops 33832960 | bytes 1220736 | tf_op jit(solution)/shard_map/dot_general | solution.py:449
  15.3 0.2 multiply_subtract_fusion
  15.5 0.1 pad_maximum_fusion
  15.6 5.3 %fusion.24 = f32[32,2,1,128]{3,2,1,0:T(1,128)S(1)} fusion(f32[32,2,128,1]{2,3,1,0:T(1,128)S(1)} %bitcast.28, f32[32,2,128,128]{3,2,1,0:T(8,128)} %param.28), kind=kOutput, calls=%fused_computation.51 | convolution fusion | flops 12582912 | bytes 4259840 | tf_op jit(solution)/shard_map/shd,shde->she/dot_general | solution.py:44
  20.9 0.2 fusion.23
  21.2 0.2 multiply_reduce_fusion
  21.4 0.1 subtract_multiply_fusion
  21.5 0.0 copy-done
  21.5 0.0 copy-done.1
  21.5 0.0 copy-done.2
  21.5 1.5 %convolution_convert_fusion.part_ref = bf16[32,2048]{1,0:T(8,128)(2,1)} fusion(bf16[256,2048]{1,0:T(8,128)(2,1)S(1)} %copy-done, f32[4,8,2,128]{3,2,1,0:T(2,128)S(1)} %bitcast.26, bf16[2048,256]{1,0:T(8,128)(2,1)S(1)} %copy-done.2, f32[256]{0:T(256)S(1)} %convert_element_type.69, bf16[32,2048]{1,0:T(8,128)(2,1)S(1)} %copy-done.1, ...), kind=kOutput, calls=%fused_computation.2 | convolution fusion | flops 67510272 | bytes 2401408 | tf_op jit(solution)/shard_map/dot_general | solution.py:463
  23.0 44.9 %tail.1 = bf16[32,512]{1,0:T(8,128)(2,1)} custom-call(bf16[32,2048]{1,0:T(8,128)(2,1)} %convolution_convert_fusion.part_ref, bf16[32,2048]{1,0:T(8,128)(2,1)} %resid_ref.1, bf16[2,2048]{1,0:T(2,128)(2,1)} %pad_maximum_fusion.1.scale_ref, bf16[8,16,32]{2,1,0:T(8,128)(2,1)} %bitcast.27, bf16[32,128]{1,0:T(8,128)(2,1)} %select_reduce_fusion.combine_ref, ...), custom_call_target="tpu_custom_call" | custom-call | tf_op jit(solution)/shard_map/tail/pallas_call | solution.py:376
  67.9 0.0 copy-start.3
  67.9 4.2 %multiply_add_fusion = f32[32,2,128,128]{3,2,1,0:T(8,128)} fusion(f32[32,2,128,128]{3,2,1,0:T(8,128)} %param.28, f32[32,2,128]{2,1,0:T(2,128)S(1)} %reshape.164, f32[32,2,128]{2,1,0:T(2,128)S(1)} %get-tuple-element.13, f32[2]{0:T(128)S(1)} %exponential_subtract_fusion), kind=kLoop, calls=%fused_computation.1 | loop fusion | flops 3145728 | bytes 8454152 | tf_op jit(solution)/shard_map/add | solution.py:49
  72.1 0.0 copy-done.3
  72.1 0.6 copy.46
  (9 shorter events, 0.1 us)
Async XLA Ops:
  0.6 20.9 %copy-start = (bf16[256,2048]{1,0:T(8,128)(2,1)S(1)}, bf16[256,2048]{1,0:T(8,128)(2,1)}, u32[]{:S(2)}) copy-start(bf16[256,2048]{1,0:T(8,128)(2,1)} %param.27) | copy-start | bytes 3145732
  11.9 9.6 %copy-start.1 = (bf16[32,2048]{1,0:T(8,128)(2,1)S(1)}, bf16[32,2048]{1,0:T(8,128)(2,1)}, u32[]{:S(2)}) copy-start(bf16[32,2048]{1,0:T(8,128)(2,1)} %resid_ref.1) | copy-start | bytes 393220
  11.9 9.6 %copy-start.2 = (bf16[2048,256]{1,0:T(8,128)(2,1)S(1)}, bf16[2048,256]{1,0:T(8,128)(2,1)}, u32[]{:S(2)}) copy-start(bf16[2048,256]{1,0:T(8,128)(2,1)} %param.25) | copy-start | bytes 3145732
  67.9 4.3 %copy-start.3 = (bf16[32,512]{1,0:T(8,128)(2,1)S(1)}, bf16[32,512]{1,0:T(8,128)(2,1)}, u32[]{:S(2)}) copy-start(bf16[32,512]{1,0:T(8,128)(2,1)} %tail.1) | copy-start | bytes 98308
where the time goes:
time: 74.1 us; the launch traced here: 72.7 us
  Pallas kernels  44.9 us (61%)
  matrix products  11.7 us (16%)
  other arithmetic  11.5 us (16%)
  local copies, waits for them, and re-layouts  3.85 us (5%)
  between operations  0.82 us (1%)
    pallas_call x1, Pallas kernels, tail(): pl.pallas_call(functools.partial(tail_kernel, tp_count, ep_count, slots),...  44.9 us
    dot_general x1, matrix products, retain(): jnp.einsum('shd,shde->she', query_rot, memory, precision=lax.Precision.HI...  5.28 us
    dot_general x3, matrix products, project(): jnp.dot(normed_in, weight, preferred_element_type=jnp.float32)  4.95 us
    add x1, other arithmetic, retain(): decays[None, :, None, None] * memory  4.25 us

commit v1 on v0

v1 whole, which is shorter than its diff:
```python
import functools

import jax
import jax.numpy as jnp
import numpy as np
from jax import lax
from jax.experimental import pallas as pl
from jax.experimental.pallas import tpu as pltpu
from jax.sharding import PartitionSpec as P

EPSILON = 1e-06
THETA = 10000.0


def rms_norm(inputs, scaling):
    square = jnp.mean(inputs * inputs, axis=-1, keepdims=True)
    return inputs * lax.rsqrt(square + EPSILON) * scaling.astype(jnp.float32)


def front_kernel(
    key_scale,
    resid_ref,
    gain_ref,
    place_ref,
    freq_ref,
    head_gain_ref,
    w_query,
    w_key,
    w_value,
    w_gate,
    state,
    out_ref,
    new_state,
    weights,
    memory,
    carried,
    weight_sem,
    load_sem,
    store_sem,
):
    f32 = jnp.float32
    bf16 = jnp.bfloat16
    seqs, heads, size, _ = memory.shape
    chunks = load_sem.shape[0]
    chunk = seqs // chunks
    fetches = [
        pltpu.make_async_copy(source, weights.at[index], weight_sem.at[index])
        for index, source in enumerate((w_query, w_key, w_value, w_gate))
    ]
    loads = [
        pltpu.make_async_copy(
            state.at[pl.ds(c * chunk, chunk)], memory.at[pl.ds(c * chunk, chunk)], load_sem.at[c]
        )
        for c in range(chunks)
    ]
    stores = [
        pltpu.make_async_copy(
            memory.at[pl.ds(c * chunk, chunk)],
            new_state.at[pl.ds(c * chunk, chunk)],
            store_sem.at[c],
        )
        for c in range(chunks)
    ]
    for copy in fetches + loads:
        copy.start()
    resid = resid_ref[...].astype(f32)
    normed = rms_norm(resid, gain_ref[...].reshape(1, -1)).astype(bf16)
    places = jnp.broadcast_to(place_ref[...].astype(f32).reshape(1, seqs), (size, seqs)).T
    angles = places * freq_ref[...]
    cosine = jnp.cos(angles)
    lane = lax.broadcasted_iota(jnp.int32, (seqs, size), 1)
    sine = jnp.where(lane < size // 2, -jnp.sin(angles), jnp.sin(angles))

    def project(index):
        fetches[index].wait()
        return (
            jnp.dot(normed, weights[index], preferred_element_type=f32).astype(bf16).astype(f32)
        )

    def rotate(inputs):
        return inputs * cosine + pltpu.roll(inputs, size // 2, 1) * sine

    def split(inputs):
        return [inputs[:, h * size : (h + 1) * size] for h in range(heads)]

    query = [rotate(part) for part in split(project(0))]
    key = [rotate(part) * key_scale for part in split(project(1))]
    value = split(project(2))
    query_t = [part.T for part in query]
    key_t = [part.T for part in key]
    head_first = lax.axis_index("tp") * heads
    decays = [
        1.0 - jnp.exp2(-1.0 - 1.5 * jnp.full((1, size), head_first + h, jnp.int32).astype(f32))
        for h in range(heads)
    ]
    gating = split(project(3))
    for c in range(chunks):
        loads[c].wait()
        for s in range(c * chunk, (c + 1) * chunk):
            for h in range(heads):
                block = memory[s, h]
                carried[h, s : s + 1, :] = jnp.sum(
                    block * query_t[h][:, s : s + 1], axis=0, keepdims=True
                )
                memory[s, h] = (
                    block * decays[h] + key_t[h][:, s : s + 1] * value[h][s : s + 1, :]
                )
        stores[c].start()
    head_gain = head_gain_ref[...].astype(f32).reshape(1, -1)
    for h in range(heads):
        within = jnp.sum(query[h] * key[h], axis=-1, keepdims=True) * value[h]
        mixture = within + carried[h] * decays[h]
        centre = jnp.mean(mixture, axis=-1, keepdims=True)
        spread = jnp.mean(jnp.square(mixture - centre), axis=-1, keepdims=True)
        place = slice(h * size, (h + 1) * size)
        scaled = (mixture - centre) * lax.rsqrt(spread + EPSILON) * head_gain[:, place]
        out_ref[:, place] = (jax.nn.silu(gating[h]) * scaled).astype(bf16)
    for copy in stores:
        copy.wait()


def front(resid, norm_gain, positions, head_gain, weights, state):
    seqs, heads, size, _ = state.shape
    half = size // 2
    inverse = THETA ** (-np.arange(half, dtype=np.float64) / half)
    freq = jnp.asarray(np.concatenate([inverse, inverse])[None, :].astype(np.float32))
    chunks = min(8, seqs)
    vmem = pl.BlockSpec(memory_space=pltpu.VMEM)
    anywhere = pl.BlockSpec(memory_space=pltpu.HBM)
    return pl.pallas_call(
        functools.partial(front_kernel, size ** (-0.5)),
        out_shape=(
            jax.ShapeDtypeStruct((seqs, heads * size), jnp.bfloat16),
            jax.ShapeDtypeStruct(state.shape, jnp.float32),
        ),
        in_specs=[vmem] * 5 + [anywhere] * 5,
        out_specs=(vmem, anywhere),
        scratch_shapes=[
            pltpu.VMEM((4,) + weights[0].shape, jnp.bfloat16),
            pltpu.VMEM(state.shape, jnp.float32),
            pltpu.VMEM((heads, seqs, size), jnp.float32),
            pltpu.SemaphoreType.DMA((4,)),
            pltpu.SemaphoreType.DMA((chunks,)),
            pltpu.SemaphoreType.DMA((chunks,)),
        ],
        compiler_params=pltpu.CompilerParams(vmem_limit_bytes=40 * 1024 * 1024),
        name="front",
    )(resid, norm_gain, positions, freq, head_gain, *weights, state)


def flip(index, mask):
    result = index
    bit = 1
    while bit <= mask:
        if mask & bit:
            result = result + bit * (1 - 2 * lax.rem(lax.div(index, bit), 2))
        bit *= 2
    return result


def tail_kernel(
    tp_count,
    ep_count,
    slots,
    retained_ref,
    resid_ref,
    gain_ref,
    mix_ref,
    routes_ref,
    route_weight_ref,
    w_output,
    dense_gate,
    dense_up,
    dense_down,
    expert_gate,
    expert_up,
    expert_down,
    out_ref,
    wo,
    wg,
    wu,
    wd,
    eg,
    eu,
    ed,
    scales,
    dispatch,
    combine,
    part,
    att_rx,
    middle,
    stat_tx,
    stat_rx,
    inverses,
    rows,
    hot,
    tokens,
    token_scale,
    gu_tx,
    gu_rx,
    gu_pair,
    gu_far,
    hidden,
    eh,
    er_tx,
    er_rx,
    er_pair,
    er_far,
    do_tx,
    do_rx,
    mo_tx,
    mo_rx,
    load_sem,
    send_sem,
    recv_sem,
):
    me_t = lax.axis_index("tp")
    me_e = lax.axis_index("ep")
    seq_dev, model_width = resid_ref.shape
    width = model_width // tp_count
    block = hidden.shape[0] // tp_count
    f32 = jnp.float32
    bf16 = jnp.bfloat16

    loads = [
        pltpu.make_async_copy(source, target, load_sem.at[index])
        for index, (source, target) in enumerate(
            (
                (w_output, wo),
                (dense_gate, wg),
                (dense_up, wu),
                (expert_gate.at[0], eg),
                (expert_up.at[0], eu),
                (expert_down.at[0], ed),
                (dense_down, wd),
            )
        )
    ]
    for load in loads:
        load.start()

    def peer_t(step):
        return flip(me_t, step)

    def peer_e(step):
        return flip(me_e, step)

    tp_steps = list(range(1, tp_count))
    ep_steps = list(range(ep_count - 1, 0, -1))
    barrier = pltpu.get_barrier_semaphore()
    for step in tp_steps:
        pl.semaphore_signal(
            barrier,
            inc=1,
            device_id=(me_e, peer_t(step)),
            device_id_type=pl.DeviceIdType.MESH,
        )
    for step in ep_steps:
        pl.semaphore_signal(
            barrier,
            inc=1,
            device_id=(peer_e(step), me_t),
            device_id_type=pl.DeviceIdType.MESH,
        )

    used = [0]
    started = []

    def send(source, target, device):
        index = used[0]
        used[0] = index + 1
        copy = pltpu.make_async_remote_copy(
            src_ref=source,
            dst_ref=target,
            send_sem=send_sem.at[index],
            recv_sem=recv_sem.at[index],
            device_id=device,
            device_id_type=pl.DeviceIdType.MESH,
        )
        copy.start()
        started.append(copy)
        return copy

    def span(index, size):
        return pl.ds(pl.multiple_of(index * size, size), size)

    def dot(left, right):
        return jnp.dot(left, right, preferred_element_type=f32)

    def arrive(copies):
        for copy in copies:
            copy.wait_recv()

    half = tp_count // 2
    sibling = peer_t(1)

    def across(step):
        return peer_t(2 * step)

    def spread(at):
        return [
            send(at(me_t), at(me_t), (me_e, target))
            for target in [sibling] + [across(k) for k in range(1, half)]
        ]

    def pass_on(copies, at):
        waiting = [copies[0]]
        for k in range(1, half):
            copies[k].wait_recv()
            waiting.append(send(at(across(k)), at(across(k)), (me_e, sibling)))
        return waiting

    own = span(me_t, width)
    scales[0:1, :] = gain_ref[...].astype(f32).reshape(1, -1)
    scales[1:2, :] = mix_ref[...].astype(f32).reshape(1, -1)
    gain = scales[0:1, own]
    mix = scales[1:2, own]

    top_count = routes_ref.shape[0]
    expert_ids = lax.broadcasted_iota(jnp.int32, (ep_count, seq_dev), 0)
    taken = jnp.zeros((ep_count, seq_dev), f32)
    weight_of = jnp.zeros((ep_count, seq_dev), f32)
    for j in range(top_count):
        named = routes_ref[j : j + 1, :] == expert_ids
        taken = taken + jnp.where(named, 1.0, 0.0)
        weight_of = weight_of + jnp.where(
            named, route_weight_ref[j : j + 1, :].astype(f32), 0.0
        )
    earlier = lax.broadcasted_iota(jnp.int32, (seq_dev, seq_dev), 0)
    later = lax.broadcasted_iota(jnp.int32, (seq_dev, seq_dev), 1)
    ranks = dot(taken.astype(bf16), jnp.where(earlier < later, 1.0, 0.0).astype(bf16))
    slot_ids = lax.broadcasted_iota(jnp.int32, (slots, seq_dev), 0).astype(f32)
    for e in range(ep_count):
        hits = (ranks[e : e + 1, :] == slot_ids) & (taken[e : e + 1, :] > 0.0)
        dispatch[e] = jnp.where(hits, 1.0, 0.0).astype(bf16)
        combine[e * slots : (e + 1) * slots, :] = jnp.where(
            hits, weight_of[e : e + 1, :], 0.0
        ).astype(bf16)

    loads[0].wait()
    retained = retained_ref[...]
    for d in tp_steps[1:] + tp_steps[:1] + [0]:
        part[d] = dot(retained, wo[:, span(peer_t(d), width)]).astype(bf16)
    pl.semaphore_wait(barrier, tp_count - 1 + ep_count - 1)
    att = [
        send(part.at[d], att_rx.at[d - 1], (me_e, peer_t(d)))
        for d in tp_steps[1:] + tp_steps[:1]
    ]
    hots = [send(dispatch.at[peer_e(d)], hot.at[me_e], (peer_e(d), me_t)) for d in ep_steps]
    hot[me_e] = dispatch[me_e]
    arrive(att)
    total = part[0].astype(f32)
    for d in tp_steps:
        total = total + att_rx[d - 1].astype(f32)
    mid = resid_ref[:, own].astype(f32) + total
    scaled = mid * gain
    rows[me_e] = scaled.astype(bf16)
    gathered = [send(rows.at[me_e], rows.at[me_e], (peer_e(d), me_t)) for d in ep_steps]
    middle[...] = mid

    lane = lax.broadcasted_iota(jnp.int32, (seq_dev, 128), 1)
    diagonal = lane == lax.broadcasted_iota(jnp.int32, (seq_dev, 128), 0)

    def to_row(column):
        return jnp.sum(jnp.where(diagonal, column, 0.0), axis=0, keepdims=True)

    def to_column(row):
        return jnp.sum(jnp.where(diagonal, row, 0.0), axis=1, keepdims=True)

    stat_tx[0:1, :] = to_row(jnp.sum(mid * mid, axis=-1, keepdims=True))
    stat_tx[1:2, :] = to_row(jnp.sum(scaled * mix, axis=-1, keepdims=True))
    stats = [send(stat_tx, stat_rx.at[d - 1], (me_e, peer_t(d))) for d in tp_steps]
    arrive(stats)
    stat = stat_tx[0:2, :]
    for d in tp_steps:
        stat = stat + stat_rx[d - 1, 0:2, :]
    inverse = lax.rsqrt(stat[0:1, :] / model_width + EPSILON)
    mixing = to_column(jax.nn.sigmoid(inverse * stat[1:2, :]))
    inverses[me_e, 0:1, :] = inverse
    factors = [
        send(inverses.at[me_e], inverses.at[me_e], (peer_e(d), me_t)) for d in ep_steps
    ]

    arrive(hots)
    arrive(gathered)
    for s in range(ep_count):
        tokens[me_t, s * slots : (s + 1) * slots, :] = dot(hot[s], rows[s]).astype(bf16)
    toks = spread(lambda index: tokens.at[index])
    near = []
    all_rows = rows[...].reshape(ep_count * seq_dev, width)
    for which, weight in enumerate((wg, wu)):
        loads[1 + which].wait()
        gu_tx[which] = lax.dot_general(
            all_rows, weight[...], (((1,), (1,)), ((), ())), preferred_element_type=f32
        ).astype(bf16)
        near.append(
            [
                send(
                    gu_tx.at[which, span(flip(sibling, 2 * k), block), :],
                    gu_rx.at[which, k],
                    (me_e, sibling),
                )
                for k in range(half)
            ]
        )
    toks = pass_on(toks, lambda index: tokens.at[index])
    far = []
    for which in range(2):
        arrive(near[which])
        for k in range(1, half):
            target = across(k)
            gu_pair[which, k - 1] = (
                gu_tx[which, span(target, block), :].astype(f32) + gu_rx[which, k].astype(f32)
            ).astype(bf16)
            far.append(
                send(gu_pair.at[which, k - 1], gu_far.at[which, k - 1], (me_e, target))
            )
    arrive(factors)
    for s in range(ep_count):
        token_scale[s * slots : (s + 1) * slots, :] = jnp.sum(
            hot[s].astype(f32) * inverses[s, 0:1, 0:seq_dev], axis=1, keepdims=True
        )
    loads[3].wait()
    loads[4].wait()
    arrive(toks)
    tile = min(256, eg.shape[1])

    def expert_tile(index, carry):
        columns = span(index, tile)
        gate = jnp.zeros((tokens.shape[1], tile), f32)
        up = jnp.zeros((tokens.shape[1], tile), f32)
        for c in range(tp_count):
            features = slice(c * width, (c + 1) * width)
            gate = gate + dot(tokens[c], eg[features, columns])
            up = up + dot(tokens[c], eu[features, columns])
        factor = token_scale[...]
        eh[:, columns] = (jax.nn.silu(gate * factor) * (up * factor)).astype(bf16)
        return carry

    lax.fori_loop(0, eg.shape[1] // tile, expert_tile, 0)

    arrive(far)
    factor = jnp.concatenate(
        [
            to_column(inverses[me_t * (block // seq_dev) + i, 0:1, :])
            for i in range(block // seq_dev)
        ],
        axis=0,
    )
    gate = gu_tx[0, span(me_t, block), :].astype(f32) + gu_rx[0, 0].astype(f32)
    up = gu_tx[1, span(me_t, block), :].astype(f32) + gu_rx[1, 0].astype(f32)
    for k in range(1, half):
        gate = gate + gu_far[0, k - 1].astype(f32)
        up = up + gu_far[1, k - 1].astype(f32)
    hidden[span(me_t, block), :] = (jax.nn.silu(gate * factor) * (up * factor)).astype(bf16)
    hids = spread(lambda index: hidden.at[span(index, block), :])
    loads[5].wait()
    pairs = []
    for k in range(half):
        target = flip(sibling, 2 * k)
        er_tx[k] = dot(eh[...], ed[:, span(target, width)]).astype(bf16)
        pairs.append(send(er_tx.at[k], er_rx.at[k], (me_e, sibling)))
    hids = pass_on(hids, lambda index: hidden.at[span(index, block), :])
    partials = []
    for k in range(1, half):
        target = across(k)
        summed = dot(eh[...], ed[:, span(target, width)])
        arrive(pairs[k : k + 1])
        er_pair[k - 1] = (summed + er_rx[k].astype(f32)).astype(bf16)
        partials.append(send(er_pair.at[k - 1], er_far.at[k - 1], (me_e, target)))
    loads[6].wait()
    arrive(hids)
    do_tx[...] = dot(hidden[...], wd[...]).astype(bf16)
    outs = [
        send(do_tx.at[span(peer_e(d), seq_dev), :], do_rx.at[d - 1], (peer_e(d), me_t))
        for d in ep_steps
    ]
    result = dot(eh[...], ed[:, own])
    arrive(pairs[:1])
    result = result + er_rx[0].astype(f32)
    arrive(partials)
    for k in range(1, half):
        result = result + er_far[k - 1].astype(f32)
    mo_tx[...] = result.astype(bf16)
    place = span(me_e, slots)
    backs = [
        send(mo_tx.at[span(peer_e(d), slots), :], mo_rx.at[place, :], (peer_e(d), me_t))
        for d in ep_steps
    ]
    mo_rx[place, :] = mo_tx[place, :]
    arrive(outs)
    dense = do_tx[span(me_e, seq_dev), :].astype(f32)
    for d in ep_steps:
        dense = dense + do_rx[d - 1].astype(f32)
    partly = middle[...] + mixing * dense
    arrive(backs)
    returned = lax.dot_general(
        combine[...], mo_rx[...], (((0,), (0,)), ((), ())), preferred_element_type=f32
    )
    out_ref[...] = (partly + returned).astype(bf16)
    for copy in started:
        copy.wait_send()


def tail(retained, resid, gain, mix, routes, route_weight, slots, weights, tp_count, ep_count):
    seq_dev, model_width = resid.shape
    width = model_width // tp_count
    batch = seq_dev * ep_count
    block = batch // tp_count
    dense_units = weights[1].shape[0]
    half = tp_count // 2
    expert_units = weights[4].shape[2]
    items = ep_count * slots
    bf16 = jnp.bfloat16
    f32 = jnp.float32
    peers_t = tp_count - 1
    peers_e = ep_count - 1
    copies = 7 * peers_t + 5 * peers_e
    vmem = pl.BlockSpec(memory_space=pltpu.VMEM)
    anywhere = pl.BlockSpec(memory_space=pltpu.HBM)
    return pl.pallas_call(
        functools.partial(tail_kernel, tp_count, ep_count, slots),
        out_shape=jax.ShapeDtypeStruct((seq_dev, width), bf16),
        in_specs=[vmem] * 6 + [anywhere] * 7,
        out_specs=vmem,
        scratch_shapes=[
            pltpu.VMEM(weights[0].shape, bf16),
            pltpu.VMEM(weights[1].shape, bf16),
            pltpu.VMEM(weights[2].shape, bf16),
            pltpu.VMEM(weights[3].shape, bf16),
            pltpu.VMEM(weights[4].shape[1:], bf16),
            pltpu.VMEM(weights[5].shape[1:], bf16),
            pltpu.VMEM(weights[6].shape[1:], bf16),
            pltpu.VMEM((8, model_width), f32),
            pltpu.VMEM((ep_count, slots, seq_dev), bf16),
            pltpu.VMEM((items, seq_dev), bf16),
            pltpu.VMEM((tp_count, seq_dev, width), bf16),
            pltpu.VMEM((peers_t, seq_dev, width), bf16),
            pltpu.VMEM((seq_dev, width), f32),
            pltpu.VMEM((8, 128), f32),
            pltpu.VMEM((peers_t, 8, 128), f32),
            pltpu.VMEM((ep_count, 8, 128), f32),
            pltpu.VMEM((ep_count, seq_dev, width), bf16),
            pltpu.VMEM((ep_count, slots, seq_dev), bf16),
            pltpu.VMEM((tp_count, items, width), bf16),
            pltpu.VMEM((items, 1), f32),
            pltpu.VMEM((2, batch, dense_units), bf16),
            pltpu.VMEM((2, half, block, dense_units), bf16),
            pltpu.VMEM((2, half - 1, block, dense_units), bf16),
            pltpu.VMEM((2, half - 1, block, dense_units), bf16),
            pltpu.VMEM((batch, dense_units), bf16),
            pltpu.VMEM((items, expert_units), bf16),
            pltpu.VMEM((half, items, width), bf16),
            pltpu.VMEM((half, items, width), bf16),
            pltpu.VMEM((half - 1, items, width), bf16),
            pltpu.VMEM((half - 1, items, width), bf16),
            pltpu.VMEM((batch, width), bf16),
            pltpu.VMEM((peers_e, seq_dev, width), bf16),
            pltpu.VMEM((items, width), bf16),
            pltpu.VMEM((items, width), bf16),
            pltpu.SemaphoreType.DMA((7,)),
            pltpu.SemaphoreType.DMA((copies,)),
            pltpu.SemaphoreType.DMA((copies,)),
        ],
        compiler_params=pltpu.CompilerParams(
            collective_id=0, has_side_effects=True, vmem_limit_bytes=61 * 1024 * 1024
        ),
        name="tail",
    )(retained, resid, gain, mix, routes, route_weight, *weights)


def per_device(
    resid,
    norm_gain,
    w_query,
    w_key,
    w_value,
    w_gate,
    head_gain,
    w_output,
    state,
    positions,
    ffn_gain,
    w_mix,
    dense_gate,
    dense_up,
    dense_down,
    routes,
    route_weight,
    expert_gate,
    expert_up,
    expert_down,
):
    seq_dev = resid.shape[0]
    tp_count = lax.axis_size("tp")
    ep_count = lax.axis_size("ep")
    retained, new_state = front(
        resid, norm_gain, positions, head_gain, (w_query, w_key, w_value, w_gate), state
    )
    capacity = max(2, 2 * seq_dev * routes.shape[1] // ep_count)
    slots = -(-capacity // 16) * 16
    final = tail(
        retained,
        resid,
        ffn_gain,
        w_mix,
        routes.T,
        route_weight.T,
        slots,
        (w_output, dense_gate.T, dense_up.T, dense_down, expert_gate, expert_up, expert_down),
        tp_count,
        ep_count,
    )
    return (final, new_state)


def solution(mesh):
    in_specs = (
        P("ep", None),
        P(),
        P(None, "tp"),
        P(None, "tp"),
        P(None, "tp"),
        P(None, "tp"),
        P("tp"),
        P("tp", None),
        P("ep", "tp", None, None),
        P("ep"),
        P(),
        P(),
        P("tp", "ep"),
        P("tp", "ep"),
        P("ep", "tp"),
        P("ep", None),
        P("ep", None),
        P("ep", None, "tp"),
        P("ep", None, "tp"),
        P("ep", "tp", None),
    )
    out_specs = (P("ep", "tp"), P("ep", "tp", None, None))
    return jax.shard_map(
        per_device, mesh=mesh, in_specs=in_specs, out_specs=out_specs, check_vma=False
    )
```

time: 74.1 us -> 63.3 us (0.85)
  matrix products: 11.7 us -> 0 us
  other arithmetic: 11.5 us -> 0 us
  local copies, waits for them, and re-layouts: 3.85 us -> 12.6 us
  Pallas kernels: 44.9 us -> 49.3 us
    dot_general x5 -> x0, matrix products: 11.7 us -> none  [the longest x1 5.28 us: retain(): jnp.einsum('shd,shde->she', query_rot, memory, precision=lax.Precision.HI...]
    unnamed x10 -> x23, local copies, waits for them, and re-layouts: 1.4 us -> 12.6 us
    pallas_call x0 -> x1, Pallas kernels: none -> 6.35 us  [front(): pl.pallas_call(functools.partial(front_kernel, size ** (-0.5)), out_shape...]
    add x2 -> x0, other arithmetic: 4.94 us -> none  [the longest x1 4.25 us: retain(): decays[None, :, None, None] * memory]
    convert_element_type x6 -> x0, other arithmetic: 2.84 us -> none  [the longest x1 0.74 us: rotate(): angles = places.astype(jnp.float32)[:, None] * inverse[None, :]]
    reduce_sum x4 -> x0, other arithmetic: 2.07 us -> none  [the longest x1 1.04 us: rms_norm(): square = jnp.mean(inputs * inputs, axis=-1, keepdims=True)]
    pallas_call x1, Pallas kernels: 44.9 us -> 43 us  [tail(): pl.pallas_call(functools.partial(tail_kernel, tp_count, ep_count, slots),...]
    another operation x2 -> x0, local copies, waits for them, and re-layouts: 1.39 us -> none  [per_device(): jnp.stack([ffn_gain, w_mix])]
where the time goes in v1:
time: 63.3 us; the launch traced here: 62.6 us
  Pallas kernels  49.3 us (78%)
  local copies, waits for them, and re-layouts  12.6 us (20%)
  between operations  0.67 us (1%)
    pallas_call x1, Pallas kernels, tail(): pl.pallas_call(functools.partial(tail_kernel, tp_count, ep_count, slots),...  43 us
    unnamed x23, local copies, waits for them, and re-layouts  12.6 us
    pallas_call x1, Pallas kernels, front(): pl.pallas_call(functools.partial(front_kernel, size ** (-0.5)), out_shape...  6.35 us

profile of v1, /device:TPU:0, one launch (start us, length us, event | category | flops | bytes accessed | tf_op | source)
XLA Modules:
  0.0 62.6 jit_solution(3108974322198123429)
XLA Ops:
  0.6 0.0 copy-start
  0.6 2.2 %copy-done = f32[32,2,128,128]{3,2,1,0:T(8,128)S(1)} copy-done((f32[32,2,128,128]{3,2,1,0:T(8,128)S(1)}, f32[32,2,128,128]{3,2,1,0:T(8,128)}, u32[]{:S(2)}) %copy-start) | copy-done | bytes 4194328
  2.8 0.0 copy-start.1
  2.8 1.2 %copy-done.1 = bf16[2048,256]{1,0:T(8,128)(2,1)S(1)} copy-done((bf16[2048,256]{1,0:T(8,128)(2,1)S(1)}, bf16[2048,256]{1,0:T(8,128)(2,1)}, u32[]{:S(2)}) %copy-start.1) | copy-done | bytes 1048600
  4.0 0.0 copy-start.2
  4.0 1.2 %copy-done.2 = bf16[2048,256]{1,0:T(8,128)(2,1)S(1)} copy-done((bf16[2048,256]{1,0:T(8,128)(2,1)S(1)}, bf16[2048,256]{1,0:T(8,128)(2,1)}, u32[]{:S(2)}) %copy-start.2) | copy-done | bytes 1048600
  5.3 0.0 copy-start.3
  5.3 1.2 %copy-done.3 = bf16[2048,256]{1,0:T(8,128)(2,1)S(1)} copy-done((bf16[2048,256]{1,0:T(8,128)(2,1)S(1)}, bf16[2048,256]{1,0:T(8,128)(2,1)}, u32[]{:S(2)}) %copy-start.3) | copy-done | bytes 1048600
  6.5 0.0 copy-start.4
  6.5 1.2 %copy-done.4 = bf16[2048,256]{1,0:T(8,128)(2,1)S(1)} copy-done((bf16[2048,256]{1,0:T(8,128)(2,1)S(1)}, bf16[2048,256]{1,0:T(8,128)(2,1)}, u32[]{:S(2)}) %copy-start.4) | copy-done | bytes 1048600
  7.7 0.0 copy-start.5
  7.7 0.9 %copy-done.5 = bf16[32,2048]{1,0:T(8,128)(2,1)S(1)} copy-done((bf16[32,2048]{1,0:T(8,128)(2,1)S(1)}, bf16[32,2048]{1,0:T(8,128)(2,1)}, u32[]{:S(2)}) %copy-start.5) | copy-done | bytes 131096
  8.6 0.0 copy-start.7
  8.6 0.7 %copy-done.7 = bf16[2048]{0:T(1024)(128)(2,1)S(1)} copy-done((bf16[2048]{0:T(1024)(128)(2,1)S(1)}, bf16[2048]{0:T(1024)(128)(2,1)}, u32[]{:S(2)}) %copy-start.7) | copy-done | bytes 4120
  9.3 0.0 copy-start.8
  9.3 0.7 %copy-done.8 = s32[32]{0:T(128)S(1)} copy-done((s32[32]{0:T(128)S(1)}, s32[32]{0:T(128)}, u32[]{:S(2)}) %copy-start.8) | copy-done | bytes 152
  10.0 0.0 copy-start.9
  10.0 0.7 %copy-done.9 = bf16[256]{0:T(256)(128)(2,1)S(1)} copy-done((bf16[256]{0:T(256)(128)(2,1)S(1)}, bf16[256]{0:T(256)(128)(2,1)}, u32[]{:S(2)}) %copy-start.9) | copy-done | bytes 536
  10.6 0.0 copy-start.10
  10.6 0.7 %copy-done.10 = f32[1,128]{1,0:T(1,128)S(1)} copy-done((f32[1,128]{1,0:T(1,128)S(1)}, f32[1,128]{1,0:T(1,128)}, u32[]{:S(2)}) %copy-start.10) | copy-done | bytes 536
  11.3 6.3 %front.1 = (bf16[32,256]{1,0:T(8,128)(2,1)S(1)}, f32[32,2,128,128]{3,2,1,0:T(8,128)}) custom-call(bf16[32,2048]{1,0:T(8,128)(2,1)S(1)} %copy-done.5, bf16[2048]{0:T(1024)(128)(2,1)S(1)} %copy-done.7, s32[32]{0:T(128)S(1)} %copy-done.8, f32[1,128]{1,0:T(1,128)S(1)} %copy-done.10, bf16[256]{0:T(256)(128)(2,1)S(1)} %copy-done.9, ...), custom_call_target="tpu_custom_call" | custom-call | tf_op jit(solution)/shard_map/front/pallas_call | solution.py:130
  17.6 0.0 copy-start.6
  17.7 0.6 copy-done.6
  18.2 43.0 %tail.1 = bf16[32,512]{1,0:T(8,128)(2,1)} custom-call(bf16[32,256]{1,0:T(8,128)(2,1)} %copy-done.6, bf16[32,2048]{1,0:T(8,128)(2,1)} %resid_ref.3, bf16[2048]{0:T(1024)(128)(2,1)} %gain_ref.3, bf16[2048]{0:T(1024)(128)(2,1)} %mix_ref.1, s32[2,32]{1,0:T(2,128)} %bitcast.6, bf16[2,32]{1,0:T(2,128)(2,1)} %bitcast.7, bf16[256,2048]{1,0:T(8,128)(2,1)} %w_output.1, ...), custom_call_target="tpu_custom_call" | custom-call | tf_op jit(solution)/shard_map/tail/pallas_call | solution.py:521
  61.2 1.4 %copy.24 = bf16[32,512]{1,0:T(8,128)(2,1)} copy(bf16[32,512]{1,0:T(8,128)(2,1)} %tail.1) | data formatting | bytes 65536
Async XLA Ops:
  0.6 2.2 %copy-start = (f32[32,2,128,128]{3,2,1,0:T(8,128)S(1)}, f32[32,2,128,128]{3,2,1,0:T(8,128)}, u32[]{:S(2)}) copy-start(f32[32,2,128,128]{3,2,1,0:T(8,128)} %state.1) | copy-start | bytes 12582916
  2.8 1.2 %copy-start.1 = (bf16[2048,256]{1,0:T(8,128)(2,1)S(1)}, bf16[2048,256]{1,0:T(8,128)(2,1)}, u32[]{:S(2)}) copy-start(bf16[2048,256]{1,0:T(8,128)(2,1)} %w_query.1) | copy-start | bytes 3145732
  4.0 1.2 %copy-start.2 = (bf16[2048,256]{1,0:T(8,128)(2,1)S(1)}, bf16[2048,256]{1,0:T(8,128)(2,1)}, u32[]{:S(2)}) copy-start(bf16[2048,256]{1,0:T(8,128)(2,1)} %w_key.1) | copy-start | bytes 3145732
  5.3 1.2 %copy-start.3 = (bf16[2048,256]{1,0:T(8,128)(2,1)S(1)}, bf16[2048,256]{1,0:T(8,128)(2,1)}, u32[]{:S(2)}) copy-start(bf16[2048,256]{1,0:T(8,128)(2,1)} %w_value.1) | copy-start | bytes 3145732
  6.5 1.2 %copy-start.4 = (bf16[2048,256]{1,0:T(8,128)(2,1)S(1)}, bf16[2048,256]{1,0:T(8,128)(2,1)}, u32[]{:S(2)}) copy-start(bf16[2048,256]{1,0:T(8,128)(2,1)} %w_gate.1) | copy-start | bytes 3145732
  7.7 0.9 %copy-start.5 = (bf16[32,2048]{1,0:T(8,128)(2,1)S(1)}, bf16[32,2048]{1,0:T(8,128)(2,1)}, u32[]{:S(2)}) copy-start(bf16[32,2048]{1,0:T(8,128)(2,1)} %resid_ref.3) | copy-start | bytes 393220
  8.6 0.7 %copy-start.7 = (bf16[2048]{0:T(1024)(128)(2,1)S(1)}, bf16[2048]{0:T(1024)(128)(2,1)}, u32[]{:S(2)}) copy-start(bf16[2048]{0:T(1024)(128)(2,1)} %gain_ref.2) | copy-start | bytes 12292
  9.3 0.7 %copy-start.8 = (s32[32]{0:T(128)S(1)}, s32[32]{0:T(128)}, u32[]{:S(2)}) copy-start(s32[32]{0:T(128)} %place_ref.1) | copy-start | bytes 388
  10.0 0.7 %copy-start.9 = (bf16[256]{0:T(256)(128)(2,1)S(1)}, bf16[256]{0:T(256)(128)(2,1)}, u32[]{:S(2)}) copy-start(bf16[256]{0:T(256)(128)(2,1)} %head_gain_ref.1) | copy-start | bytes 1540
  10.6 0.7 %copy-start.10 = (f32[1,128]{1,0:T(1,128)S(1)}, f32[1,128]{1,0:T(1,128)}, u32[]{:S(2)}) copy-start(f32[1,128]{1,0:T(1,128)} %constant.2.clone.freq_ref) | copy-start | bytes 1540
  17.6 0.6 copy-start.6

commit v2 on v1

--- a/solution.py
+++ b/solution.py
@@ -19,11 +19,11 @@
 
 def front_kernel(
     key_scale,
-    resid_ref,
-    gain_ref,
-    place_ref,
-    freq_ref,
-    head_gain_ref,
+    resid,
+    norm_gain,
+    positions,
+    freq,
+    head_gain,
     w_query,
     w_key,
     w_value,
@@ -31,9 +31,15 @@
     state,
     out_ref,
     new_state,
+    resid_ref,
+    gain_ref,
+    place_ref,
+    freq_ref,
+    head_gain_ref,
     weights,
     memory,
     carried,
+    small_sem,
     weight_sem,
     load_sem,
     store_sem,
@@ -43,6 +49,18 @@
     seqs, heads, size, _ = memory.shape
     chunks = load_sem.shape[0]
     chunk = seqs // chunks
+    smalls = [
+        pltpu.make_async_copy(source, target, small_sem.at[index])
+        for index, (source, target) in enumerate(
+            (
+                (resid, resid_ref),
+                (norm_gain, gain_ref),
+                (positions, place_ref),
+                (freq, freq_ref),
+                (head_gain, head_gain_ref),
+            )
+        )
+    ]
     fetches = [
         pltpu.make_async_copy(source, weights.at[index], weight_sem.at[index])
         for index, source in enumerate((w_query, w_key, w_value, w_gate))
@@ -61,8 +79,10 @@
         )
         for c in range(chunks)
     ]
-    for copy in fetches + loads:
+    for copy in smalls + fetches + loads:
         copy.start()
+    for copy in smalls:
+        copy.wait()
     resid = resid_ref[...].astype(f32)
     normed = rms_norm(resid, gain_ref[...].reshape(1, -1)).astype(bf16)
     places = jnp.broadcast_to(place_ref[...].astype(f32).reshape(1, seqs), (size, seqs)).T
@@ -106,14 +126,14 @@
                     block * decays[h] + key_t[h][:, s : s + 1] * value[h][s : s + 1, :]
                 )
         stores[c].start()
-    head_gain = head_gain_ref[...].astype(f32).reshape(1, -1)
+    gains = head_gain_ref[...].astype(f32).reshape(1, -1)
     for h in range(heads):
         within = jnp.sum(query[h] * key[h], axis=-1, keepdims=True) * value[h]
         mixture = within + carried[h] * decays[h]
         centre = jnp.mean(mixture, axis=-1, keepdims=True)
         spread = jnp.mean(jnp.square(mixture - centre), axis=-1, keepdims=True)
         place = slice(h * size, (h + 1) * size)
-        scaled = (mixture - centre) * lax.rsqrt(spread + EPSILON) * head_gain[:, place]
+        scaled = (mixture - centre) * lax.rsqrt(spread + EPSILON) * gains[:, place]
         out_ref[:, place] = (jax.nn.silu(gating[h]) * scaled).astype(bf16)
     for copy in stores:
         copy.wait()
@@ -133,17 +153,23 @@
             jax.ShapeDtypeStruct((seqs, heads * size), jnp.bfloat16),
             jax.ShapeDtypeStruct(state.shape, jnp.float32),
         ),
-        in_specs=[vmem] * 5 + [anywhere] * 5,
+        in_specs=[anywhere] * 10,
         out_specs=(vmem, anywhere),
         scratch_shapes=[
+            pltpu.VMEM(resid.shape, resid.dtype),
+            pltpu.VMEM(norm_gain.shape, norm_gain.dtype),
+            pltpu.VMEM(positions.shape, positions.dtype),
+            pltpu.VMEM(freq.shape, freq.dtype),
+            pltpu.VMEM(head_gain.shape, head_gain.dtype),
             pltpu.VMEM((4,) + weights[0].shape, jnp.bfloat16),
             pltpu.VMEM(state.shape, jnp.float32),
             pltpu.VMEM((heads, seqs, size), jnp.float32),
+            pltpu.SemaphoreType.DMA((5,)),
             pltpu.SemaphoreType.DMA((4,)),
             pltpu.SemaphoreType.DMA((chunks,)),
             pltpu.SemaphoreType.DMA((chunks,)),
         ],
-        compiler_params=pltpu.CompilerParams(vmem_limit_bytes=40 * 1024 * 1024),
+        compiler_params=pltpu.CompilerParams(vmem_limit_bytes=61 * 1024 * 1024),
         name="front",
     )(resid, norm_gain, positions, freq, head_gain, *weights, state)
 
@@ -162,12 +188,12 @@
     tp_count,
     ep_count,
     slots,
-    retained_ref,
-    resid_ref,
-    gain_ref,
-    mix_ref,
-    routes_ref,
-    route_weight_ref,
+    retained,
+    resid,
+    ffn_gain,
+    w_mix,
+    routes,
+    route_weight,
     w_output,
     dense_gate,
     dense_up,
@@ -176,6 +202,12 @@
     expert_up,
     expert_down,
     out_ref,
+    retained_ref,
+    resid_ref,
+    gain_ref,
+    mix_ref,
+    routes_ref,
+    route_weight_ref,
     wo,
     wg,
     wu,
@@ -226,6 +258,12 @@
         pltpu.make_async_copy(source, target, load_sem.at[index])
         for index, (source, target) in enumerate(
             (
+                (retained, retained_ref),
+                (resid, resid_ref),
+                (ffn_gain, gain_ref),
+                (w_mix, mix_ref),
+                (routes, routes_ref),
+                (route_weight, route_weight_ref),
                 (w_output, wo),
                 (dense_gate, wg),
                 (dense_up, wu),
@@ -238,6 +276,10 @@
     ]
     for load in loads:
         load.start()
+
+    def ready(*indices):
+        for index in indices:
+            loads[index].wait()
 
     def peer_t(step):
         return flip(me_t, step)
@@ -306,11 +348,12 @@
     def pass_on(copies, at):
         waiting = [copies[0]]
         for k in range(1, half):
-            copies[k].wait_recv()
+            arrive(copies[k : k + 1])
             waiting.append(send(at(across(k)), at(across(k)), (me_e, sibling)))
         return waiting
 
     own = span(me_t, width)
+    ready(2, 3, 4, 5)
     scales[0:1, :] = gain_ref[...].astype(f32).reshape(1, -1)
     scales[1:2, :] = mix_ref[...].astype(f32).reshape(1, -1)
     gain = scales[0:1, own]
@@ -337,10 +380,10 @@
             hits, weight_of[e : e + 1, :], 0.0
         ).astype(bf16)
 
-    loads[0].wait()
-    retained = retained_ref[...]
+    ready(0, 1, 6)
+    kept = retained_ref[...]
     for d in tp_steps[1:] + tp_steps[:1] + [0]:
-        part[d] = dot(retained, wo[:, span(peer_t(d), width)]).astype(bf16)
+        part[d] = dot(kept, wo[:, span(peer_t(d), width)]).astype(bf16)
     pl.semaphore_wait(barrier, tp_count - 1 + ep_count - 1)
     att = [
         send(part.at[d], att_rx.at[d - 1], (me_e, peer_t(d)))
@@ -389,7 +432,7 @@
     near = []
     all_rows = rows[...].reshape(ep_count * seq_dev, width)
     for which, weight in enumerate((wg, wu)):
-        loads[1 + which].wait()
+        ready(7 + which)
         gu_tx[which] = lax.dot_general(
             all_rows, weight[...], (((1,), (1,)), ((), ())), preferred_element_type=f32
         ).astype(bf16)
@@ -420,8 +463,7 @@
         token_scale[s * slots : (s + 1) * slots, :] = jnp.sum(
             hot[s].astype(f32) * inverses[s, 0:1, 0:seq_dev], axis=1, keepdims=True
         )
-    loads[3].wait()
-    loads[4].wait()
+    ready(9, 10)
     arrive(toks)
     tile = min(256, eg.shape[1])
 
@@ -438,7 +480,6 @@
         return carry
 
     lax.fori_loop(0, eg.shape[1] // tile, expert_tile, 0)
-
     arrive(far)
     factor = jnp.concatenate(
         [
@@ -454,7 +495,7 @@
         up = up + gu_far[1, k - 1].astype(f32)
     hidden[span(me_t, block), :] = (jax.nn.silu(gate * factor) * (up * factor)).astype(bf16)
     hids = spread(lambda index: hidden.at[span(index, block), :])
-    loads[5].wait()
+    ready(11)
     pairs = []
     for k in range(half):
         target = flip(sibling, 2 * k)
@@ -468,7 +509,7 @@
         arrive(pairs[k : k + 1])
         er_pair[k - 1] = (summed + er_rx[k].astype(f32)).astype(bf16)
         partials.append(send(er_pair.at[k - 1], er_far.at[k - 1], (me_e, target)))
-    loads[6].wait()
+    ready(12)
     arrive(hids)
     do_tx[...] = dot(hidden[...], wd[...]).astype(bf16)
     outs = [
@@ -521,9 +562,15 @@
     return pl.pallas_call(
         functools.partial(tail_kernel, tp_count, ep_count, slots),
         out_shape=jax.ShapeDtypeStruct((seq_dev, width), bf16),
-        in_specs=[vmem] * 6 + [anywhere] * 7,
+        in_specs=[anywhere] * 13,
         out_specs=vmem,
         scratch_shapes=[
+            pltpu.VMEM(retained.shape, bf16),
+            pltpu.VMEM(resid.shape, bf16),
+            pltpu.VMEM(gain.shape, bf16),
+            pltpu.VMEM(mix.shape, bf16),
+            pltpu.VMEM(routes.shape, jnp.int32),
+            pltpu.VMEM(route_weight.shape, bf16),
             pltpu.VMEM(weights[0].shape, bf16),
             pltpu.VMEM(weights[1].shape, bf16),
             pltpu.VMEM(weights[2].shape, bf16),
@@ -558,7 +605,7 @@
             pltpu.VMEM((peers_e, seq_dev, width), bf16),
             pltpu.VMEM((items, width), bf16),
             pltpu.VMEM((items, width), bf16),
-            pltpu.SemaphoreType.DMA((7,)),
+            pltpu.SemaphoreType.DMA((13,)),
             pltpu.SemaphoreType.DMA((copies,)),
             pltpu.SemaphoreType.DMA((copies,)),
         ],

time: 63.3 us -> 53.8 us (0.85)
  local copies, waits for them, and re-layouts: 12.6 us -> 1.38 us
  Pallas kernels: 49.3 us -> 51.4 us
    unnamed x23 -> x1, local copies, waits for them, and re-layouts: 12.6 us -> 1.38 us
    pallas_call x1, Pallas kernels: 6.35 us -> 9.18 us  [front(): pl.pallas_call(functools.partial(front_kernel, size ** (-0.5)), out_shape...]
    pallas_call x1, Pallas kernels: 43 us -> 42.2 us  [tail(): pl.pallas_call(functools.partial(tail_kernel, tp_count, ep_count, slots),...]
where the time goes in v2:
time: 53.8 us; the launch traced here: 53.4 us
  Pallas kernels  51.4 us (96%)
  local copies, waits for them, and re-layouts  1.38 us (3%)
  between operations  0.65 us (1%)
    pallas_call x1, Pallas kernels, tail(): pl.pallas_call(functools.partial(tail_kernel, tp_count, ep_count, slots),...  42.2 us
    pallas_call x1, Pallas kernels, front(): pl.pallas_call(functools.partial(front_kernel, size ** (-0.5)), out_shape...  9.18 us
    unnamed x1, local copies, waits for them, and re-layouts  1.38 us

profile of v2, /device:TPU:0, one launch (start us, length us, event | category | flops | bytes accessed | tf_op | source)
XLA Modules:
  0.0 53.4 jit_solution(8233610307376233510)
XLA Ops:
  0.6 9.2 %front.1 = (bf16[32,256]{1,0:T(8,128)(2,1)}, f32[32,2,128,128]{3,2,1,0:T(8,128)}) custom-call(bf16[32,2048]{1,0:T(8,128)(2,1)} %resid.3, bf16[2048]{0:T(1024)(128)(2,1)} %norm_gain.1, s32[32]{0:T(128)} %positions.1, f32[1,128]{1,0:T(1,128)} %constant.2.clone.freq, bf16[256]{0:T(256)(128)(2,1)} %head_gain.1, bf16[2048,256]{1,0:T(8,128)(2,1)} %w_query.1, ...), custom_call_target="tpu_custom_call" | custom-call | tf_op jit(solution)/shard_map/front/pallas_call | solution.py:150
  9.8 42.2 %tail.1 = bf16[32,512]{1,0:T(8,128)(2,1)} custom-call(bf16[32,256]{1,0:T(8,128)(2,1)} %get-tuple-element.4.retained, bf16[32,2048]{1,0:T(8,128)(2,1)} %resid.3, bf16[2048]{0:T(1024)(128)(2,1)} %ffn_gain.1, bf16[2048]{0:T(1024)(128)(2,1)} %w_mix.1, s32[2,32]{1,0:T(2,128)} %bitcast.6, bf16[2,32]{1,0:T(2,128)(2,1)} %bitcast.7, bf16[256,2048]{1,0:T(8,128)(2,1)} %w_output.1, ...), custom_call_target="tpu_custom_call" | custom-call | tf_op jit(solution)/shard_map/tail/pallas_call | solution.py:562
  52.1 1.4 %copy.24 = bf16[32,512]{1,0:T(8,128)(2,1)} copy(bf16[32,512]{1,0:T(8,128)(2,1)} %tail.1) | data formatting | bytes 65536

commit v3 on v1

--- a/solution.py
+++ b/solution.py
@@ -17,35 +17,29 @@
     return inputs * lax.rsqrt(square + EPSILON) * scaling.astype(jnp.float32)
 
 
-def front_kernel(
-    key_scale,
-    resid_ref,
-    gain_ref,
-    place_ref,
-    freq_ref,
-    head_gain_ref,
-    w_query,
-    w_key,
-    w_value,
-    w_gate,
+def state_kernel(
     state,
+    key,
+    value,
+    final,
+    new_state,
     out_ref,
-    new_state,
-    weights,
     memory,
-    carried,
-    weight_sem,
+    key_ref,
+    value_ref,
+    final_ref,
+    small_sem,
     load_sem,
     store_sem,
 ):
-    f32 = jnp.float32
-    bf16 = jnp.bfloat16
     seqs, heads, size, _ = memory.shape
     chunks = load_sem.shape[0]
     chunk = seqs // chunks
-    fetches = [
-        pltpu.make_async_copy(source, weights.at[index], weight_sem.at[index])
-        for index, source in enumerate((w_query, w_key, w_value, w_gate))
+    smalls = [
+        pltpu.make_async_copy(source, target, small_sem.at[index])
+        for index, (source, target) in enumerate(
+            ((key, key_ref), (value, value_ref), (final, final_ref))
+        )
     ]
     loads = [
         pltpu.make_async_copy(
@@ -61,91 +55,59 @@
         )
         for c in range(chunks)
     ]
-    for copy in fetches + loads:
+    for copy in smalls + loads:
         copy.start()
-    resid = resid_ref[...].astype(f32)
-    normed = rms_norm(resid, gain_ref[...].reshape(1, -1)).astype(bf16)
-    places = jnp.broadcast_to(place_ref[...].astype(f32).reshape(1, seqs), (size, seqs)).T
-    angles = places * freq_ref[...]
-    cosine = jnp.cos(angles)
-    lane = lax.broadcasted_iota(jnp.int32, (seqs, size), 1)
-    sine = jnp.where(lane < size // 2, -jnp.sin(angles), jnp.sin(angles))
-
-    def project(index):
-        fetches[index].wait()
-        return (
-            jnp.dot(normed, weights[index], preferred_element_type=f32).astype(bf16).astype(f32)
-        )
-
-    def rotate(inputs):
-        return inputs * cosine + pltpu.roll(inputs, size // 2, 1) * sine
-
-    def split(inputs):
-        return [inputs[:, h * size : (h + 1) * size] for h in range(heads)]
-
-    query = [rotate(part) for part in split(project(0))]
-    key = [rotate(part) * key_scale for part in split(project(1))]
-    value = split(project(2))
-    query_t = [part.T for part in query]
-    key_t = [part.T for part in key]
-    head_first = lax.axis_index("tp") * heads
-    decays = [
-        1.0 - jnp.exp2(-1.0 - 1.5 * jnp.full((1, size), head_first + h, jnp.int32).astype(f32))
-        for h in range(heads)
-    ]
-    gating = split(project(3))
+    decays = decays_of(heads, size)
+    for copy in smalls:
+        copy.wait()
+    placed = pltpu.make_async_copy(final_ref, out_ref, small_sem.at[3])
+    placed.start()
+    keys = [key_ref[h] for h in range(heads)]
     for c in range(chunks):
         loads[c].wait()
         for s in range(c * chunk, (c + 1) * chunk):
             for h in range(heads):
-                block = memory[s, h]
-                carried[h, s : s + 1, :] = jnp.sum(
-                    block * query_t[h][:, s : s + 1], axis=0, keepdims=True
-                )
                 memory[s, h] = (
-                    block * decays[h] + key_t[h][:, s : s + 1] * value[h][s : s + 1, :]
+                    memory[s, h] * decays[h]
+                    + keys[h][:, s : s + 1] * value_ref[s : s + 1, h * size : (h + 1) * size]
                 )
         stores[c].start()
-    head_gain = head_gain_ref[...].astype(f32).reshape(1, -1)
-    for h in range(heads):
-        within = jnp.sum(query[h] * key[h], axis=-1, keepdims=True) * value[h]
-        mixture = within + carried[h] * decays[h]
-        centre = jnp.mean(mixture, axis=-1, keepdims=True)
-        spread = jnp.mean(jnp.square(mixture - centre), axis=-1, keepdims=True)
-        place = slice(h * size, (h + 1) * size)
-        scaled = (mixture - centre) * lax.rsqrt(spread + EPSILON) * head_gain[:, place]
-        out_ref[:, place] = (jax.nn.silu(gating[h]) * scaled).astype(bf16)
+    placed.wait()
     for copy in stores:
         copy.wait()
 
 
-def front(resid, norm_gain, positions, head_gain, weights, state):
-    seqs, heads, size, _ = state.shape
-    half = size // 2
-    inverse = THETA ** (-np.arange(half, dtype=np.float64) / half)
-    freq = jnp.asarray(np.concatenate([inverse, inverse])[None, :].astype(np.float32))
-    chunks = min(8, seqs)
-    vmem = pl.BlockSpec(memory_space=pltpu.VMEM)
+def update_state(state, key, value, final):
+    chunks = min(8, state.shape[0])
     anywhere = pl.BlockSpec(memory_space=pltpu.HBM)
     return pl.pallas_call(
-        functools.partial(front_kernel, size ** (-0.5)),
+        state_kernel,
         out_shape=(
-            jax.ShapeDtypeStruct((seqs, heads * size), jnp.bfloat16),
             jax.ShapeDtypeStruct(state.shape, jnp.float32),
+            jax.ShapeDtypeStruct(final.shape, final.dtype),
         ),
-        in_specs=[vmem] * 5 + [anywhere] * 5,
-        out_specs=(vmem, anywhere),
+        in_specs=[anywhere] * 4,
+        out_specs=(anywhere, anywhere),
         scratch_shapes=[
-            pltpu.VMEM((4,) + weights[0].shape, jnp.bfloat16),
             pltpu.VMEM(state.shape, jnp.float32),
-            pltpu.VMEM((heads, seqs, size), jnp.float32),
+            pltpu.VMEM(key.shape, key.dtype),
+            pltpu.VMEM(value.shape, value.dtype),
+            pltpu.VMEM(final.shape, final.dtype),
             pltpu.SemaphoreType.DMA((4,)),
             pltpu.SemaphoreType.DMA((chunks,)),
             pltpu.SemaphoreType.DMA((chunks,)),
         ],
-        compiler_params=pltpu.CompilerParams(vmem_limit_bytes=40 * 1024 * 1024),
-        name="front",
-    )(resid, norm_gain, positions, freq, head_gain, *weights, state)
+        compiler_params=pltpu.CompilerParams(vmem_limit_bytes=61 * 1024 * 1024),
+        name="update_state",
+    )(state, key, value, final)
+
+
+def decays_of(heads, size):
+    head_first = lax.axis_index("tp") * heads
+    return [
+        1.0 - jnp.exp2(-1.0 - 1.5 * jnp.full((1, size), head_first + h, jnp.int32).astype(jnp.float32))
+        for h in range(heads)
+    ]
 
 
 def flip(index, mask):
@@ -158,16 +120,25 @@
     return result
 
 
-def tail_kernel(
+def layer_kernel(
     tp_count,
     ep_count,
     slots,
-    retained_ref,
-    resid_ref,
-    gain_ref,
-    mix_ref,
-    routes_ref,
-    route_weight_ref,
+    key_scale,
+    resid,
+    norm_gain,
+    positions,
+    freq,
+    head_gain,
+    ffn_gain,
+    w_mix,
+    routes,
+    route_weight,
+    w_query,
+    w_key,
+    w_value,
+    w_gate,
+    state,
     w_output,
     dense_gate,
     dense_up,
@@ -176,6 +147,21 @@
     expert_up,
     expert_down,
     out_ref,
+    key_out,
+    value_out,
+    resid_ref,
+    norm_ref,
+    place_ref,
+    freq_ref,
+    head_ref,
+    gain_ref,
+    mix_ref,
+    routes_ref,
+    route_weight_ref,
+    projections,
+    memory,
+    carried,
+    kept,
     wo,
     wg,
     wu,
@@ -210,6 +196,8 @@
     do_rx,
     mo_tx,
     mo_rx,
+    fetch_sem,
+    state_sem,
     load_sem,
     send_sem,
     recv_sem,
@@ -222,6 +210,35 @@
     f32 = jnp.float32
     bf16 = jnp.bfloat16
 
+    fetches = [
+        pltpu.make_async_copy(source, target, fetch_sem.at[index])
+        for index, (source, target) in enumerate(
+            (
+                (resid, resid_ref),
+                (norm_gain, norm_ref),
+                (positions, place_ref),
+                (freq, freq_ref),
+                (head_gain, head_ref),
+                (ffn_gain, gain_ref),
+                (w_mix, mix_ref),
+                (routes, routes_ref),
+                (route_weight, route_weight_ref),
+                (w_query, projections.at[0]),
+                (w_key, projections.at[1]),
+                (w_value, projections.at[2]),
+                (w_gate, projections.at[3]),
+            )
+        )
+    ]
+    seqs, heads, size, _ = memory.shape
+    chunks = state_sem.shape[0]
+    chunk = seqs // chunks
+    states = [
+        pltpu.make_async_copy(
+            state.at[pl.ds(c * chunk, chunk)], memory.at[pl.ds(c * chunk, chunk)], state_sem.at[c]
+        )
+        for c in range(chunks)
+    ]
     loads = [
         pltpu.make_async_copy(source, target, load_sem.at[index])
         for index, (source, target) in enumerate(
@@ -236,8 +253,12 @@
             )
         )
     ]
-    for load in loads:
-        load.start()
+    for copy in fetches + states + loads[:1]:
+        copy.start()
+
+    def ready(*indices):
+        for index in indices:
+            loads[index].wait()
 
     def peer_t(step):
         return flip(me_t, step)
@@ -306,11 +327,66 @@
     def pass_on(copies, at):
         waiting = [copies[0]]
         for k in range(1, half):
-            copies[k].wait_recv()
+            arrive(copies[k : k + 1])
             waiting.append(send(at(across(k)), at(across(k)), (me_e, sibling)))
         return waiting
 
     own = span(me_t, width)
+    for copy in fetches[:5]:
+        copy.wait()
+    normed = rms_norm(resid_ref[...].astype(f32), norm_ref[...].reshape(1, -1)).astype(bf16)
+    places = jnp.broadcast_to(place_ref[...].astype(f32).reshape(1, seqs), (size, seqs)).T
+    angles = places * freq_ref[...]
+    cosine = jnp.cos(angles)
+    lane_of = lax.broadcasted_iota(jnp.int32, (seqs, size), 1)
+    sine = jnp.where(lane_of < size // 2, -jnp.sin(angles), jnp.sin(angles))
+
+    def project(index):
+        fetches[9 + index].wait()
+        product = dot(normed, projections[index]).astype(bf16).astype(f32)
+        return [product[:, h * size : (h + 1) * size] for h in range(heads)]
+
+    def rotate(inputs):
+        return inputs * cosine + pltpu.roll(inputs, size // 2, 1) * sine
+
+    query = [rotate(piece) for piece in project(0)]
+    query_t = [piece.T for piece in query]
+    key = [rotate(piece) * key_scale for piece in project(1)]
+    value = project(2)
+    gating = project(3)
+    decays = decays_of(heads, size)
+    for h in range(heads):
+        key_out[h] = key[h].T
+        value_out[:, h * size : (h + 1) * size] = value[h]
+    for c in range(chunks):
+        states[c].wait()
+        for q in range(c * chunk, (c + 1) * chunk):
+            for h in range(heads):
+                carried[h, q : q + 1, :] = jnp.sum(
+                    memory[q, h] * query_t[h][:, q : q + 1], axis=0, keepdims=True
+                )
+    for load in loads[1:]:
+        load.start()
+    gains = head_ref[...].astype(f32).reshape(1, -1)
+    for h in range(heads):
+        within = jnp.sum(query[h] * key[h], axis=-1, keepdims=True) * value[h]
+        mixture = within + carried[h] * decays[h]
+        centre = jnp.mean(mixture, axis=-1, keepdims=True)
+        variance = jnp.mean(jnp.square(mixture - centre), axis=-1, keepdims=True)
+        columns = slice(h * size, (h + 1) * size)
+        scaled = (mixture - centre) * lax.rsqrt(variance + EPSILON) * gains[:, columns]
+        kept[:, columns] = (jax.nn.silu(gating[h]) * scaled).astype(bf16)
+    ready(0)
+    retained = kept[...]
+    for d in tp_steps[1:] + tp_steps[:1] + [0]:
+        part[d] = dot(retained, wo[:, span(peer_t(d), width)]).astype(bf16)
+    pl.semaphore_wait(barrier, tp_count - 1 + ep_count - 1)
+    att = [
+        send(part.at[d], att_rx.at[d - 1], (me_e, peer_t(d)))
+        for d in tp_steps[1:] + tp_steps[:1]
+    ]
+    for copy in fetches[5:9]:
+        copy.wait()
     scales[0:1, :] = gain_ref[...].astype(f32).reshape(1, -1)
     scales[1:2, :] = mix_ref[...].astype(f32).reshape(1, -1)
     gain = scales[0:1, own]
@@ -337,15 +413,6 @@
             hits, weight_of[e : e + 1, :], 0.0
         ).astype(bf16)
 
-    loads[0].wait()
-    retained = retained_ref[...]
-    for d in tp_steps[1:] + tp_steps[:1] + [0]:
-        part[d] = dot(retained, wo[:, span(peer_t(d), width)]).astype(bf16)
-    pl.semaphore_wait(barrier, tp_count - 1 + ep_count - 1)
-    att = [
-        send(part.at[d], att_rx.at[d - 1], (me_e, peer_t(d)))
-        for d in tp_steps[1:] + tp_steps[:1]
-    ]
     hots = [send(dispatch.at[peer_e(d)], hot.at[me_e], (peer_e(d), me_t)) for d in ep_steps]
     hot[me_e] = dispatch[me_e]
     arrive(att)
@@ -389,7 +456,7 @@
     near = []
     all_rows = rows[...].reshape(ep_count * seq_dev, width)
     for which, weight in enumerate((wg, wu)):
-        loads[1 + which].wait()
+        ready(1 + which)
         gu_tx[which] = lax.dot_general(
             all_rows, weight[...], (((1,), (1,)), ((), ())), preferred_element_type=f32
         ).astype(bf16)
@@ -420,8 +487,7 @@
         token_scale[s * slots : (s + 1) * slots, :] = jnp.sum(
             hot[s].astype(f32) * inverses[s, 0:1, 0:seq_dev], axis=1, keepdims=True
         )
-    loads[3].wait()
-    loads[4].wait()
+    ready(3, 4)
     arrive(toks)
     tile = min(256, eg.shape[1])
 
@@ -438,7 +504,12 @@
         return carry
 
     lax.fori_loop(0, eg.shape[1] // tile, expert_tile, 0)
-
+    ready(5)
+    pairs = []
+    for k in range(half):
+        target = flip(sibling, 2 * k)
+        er_tx[k] = dot(eh[...], ed[:, span(target, width)]).astype(bf16)
+        pairs.append(send(er_tx.at[k], er_rx.at[k], (me_e, sibling)))
     arrive(far)
     factor = jnp.concatenate(
         [
@@ -454,13 +525,6 @@
         up = up + gu_far[1, k - 1].astype(f32)
     hidden[span(me_t, block), :] = (jax.nn.silu(gate * factor) * (up * factor)).astype(bf16)
     hids = spread(lambda index: hidden.at[span(index, block), :])
-    loads[5].wait()
-    pairs = []
-    for k in range(half):
-        target = flip(sibling, 2 * k)
-        er_tx[k] = dot(eh[...], ed[:, span(target, width)]).astype(bf16)
-        pairs.append(send(er_tx.at[k], er_rx.at[k], (me_e, sibling)))
-    hids = pass_on(hids, lambda index: hidden.at[span(index, block), :])
     partials = []
     for k in range(1, half):
         target = across(k)
@@ -468,16 +532,17 @@
         arrive(pairs[k : k + 1])
         er_pair[k - 1] = (summed + er_rx[k].astype(f32)).astype(bf16)
         partials.append(send(er_pair.at[k - 1], er_far.at[k - 1], (me_e, target)))
-    loads[6].wait()
+    result = dot(eh[...], ed[:, own])
+    arrive(pairs[:1])
+    result = result + er_rx[0].astype(f32)
+    hids = pass_on(hids, lambda index: hidden.at[span(index, block), :])
+    ready(6)
     arrive(hids)
     do_tx[...] = dot(hidden[...], wd[...]).astype(bf16)
     outs = [
         send(do_tx.at[span(peer_e(d), seq_dev), :], do_rx.at[d - 1], (peer_e(d), me_t))
         for d in ep_steps
     ]
-    result = dot(eh[...], ed[:, own])
-    arrive(pairs[:1])
-    result = result + er_rx[0].astype(f32)
     arrive(partials)
     for k in range(1, half):
         result = result + er_far[k - 1].astype(f32)
@@ -502,8 +567,10 @@
         copy.wait_send()
 
 
-def tail(retained, resid, gain, mix, routes, route_weight, slots, weights, tp_count, ep_count):
-    seq_dev, model_width = resid.shape
+def layer(smalls, slots, projections, state, weights, tp_count, ep_count):
+    seq_dev, model_width = smalls[0].shape
+    _, heads, size, _ = state.shape
+    chunks = min(8, seq_dev)
     width = model_width // tp_count
     batch = seq_dev * ep_count
     block = batch // tp_count
@@ -519,11 +586,20 @@
     vmem = pl.BlockSpec(memory_space=pltpu.VMEM)
     anywhere = pl.BlockSpec(memory_space=pltpu.HBM)
     return pl.pallas_call(
-        functools.partial(tail_kernel, tp_count, ep_count, slots),
-        out_shape=jax.ShapeDtypeStruct((seq_dev, width), bf16),
-        in_specs=[vmem] * 6 + [anywhere] * 7,
-        out_specs=vmem,
+        functools.partial(layer_kernel, tp_count, ep_count, slots, size ** (-0.5)),
+        out_shape=(
+            jax.ShapeDtypeStruct((seq_dev, width), bf16),
+            jax.ShapeDtypeStruct((heads, size, seq_dev), f32),
+            jax.ShapeDtypeStruct((seq_dev, heads * size), f32),
+        ),
+        in_specs=[anywhere] * 21,
+        out_specs=(vmem, vmem, vmem),
         scratch_shapes=[
+            *[pltpu.VMEM(small.shape, small.dtype) for small in smalls],
+            pltpu.VMEM((4,) + projections[0].shape, bf16),
+            pltpu.VMEM(state.shape, f32),
+            pltpu.VMEM((heads, seq_dev, size), f32),
+            pltpu.VMEM((seq_dev, heads * size), bf16),
             pltpu.VMEM(weights[0].shape, bf16),
             pltpu.VMEM(weights[1].shape, bf16),
             pltpu.VMEM(weights[2].shape, bf16),
@@ -558,6 +634,8 @@
             pltpu.VMEM((peers_e, seq_dev, width), bf16),
             pltpu.VMEM((items, width), bf16),
             pltpu.VMEM((items, width), bf16),
+            pltpu.SemaphoreType.DMA((13,)),
+            pltpu.SemaphoreType.DMA((chunks,)),
             pltpu.SemaphoreType.DMA((7,)),
             pltpu.SemaphoreType.DMA((copies,)),
             pltpu.SemaphoreType.DMA((copies,)),
@@ -565,8 +643,8 @@
         compiler_params=pltpu.CompilerParams(
             collective_id=0, has_side_effects=True, vmem_limit_bytes=61 * 1024 * 1024
         ),
-        name="tail",
-    )(retained, resid, gain, mix, routes, route_weight, *weights)
+        name="layer",
+    )(*smalls, *projections, state, *weights)
 
 
 def per_device(
@@ -594,23 +672,31 @@
     seq_dev = resid.shape[0]
     tp_count = lax.axis_size("tp")
     ep_count = lax.axis_size("ep")
-    retained, new_state = front(
-        resid, norm_gain, positions, head_gain, (w_query, w_key, w_value, w_gate), state
-    )
+    half = state.shape[-1] // 2
+    inverse = THETA ** (-np.arange(half, dtype=np.float64) / half)
+    freq = jnp.asarray(np.concatenate([inverse, inverse])[None, :].astype(np.float32))
     capacity = max(2, 2 * seq_dev * routes.shape[1] // ep_count)
     slots = -(-capacity // 16) * 16
-    final = tail(
-        retained,
-        resid,
-        ffn_gain,
-        w_mix,
-        routes.T,
-        route_weight.T,
+    final, key, value = layer(
+        (
+            resid,
+            norm_gain,
+            positions,
+            freq,
+            head_gain,
+            ffn_gain,
+            w_mix,
+            routes.T,
+            route_weight.T,
+        ),
         slots,
+        (w_query, w_key, w_value, w_gate),
+        state,
         (w_output, dense_gate.T, dense_up.T, dense_down, expert_gate, expert_up, expert_down),
         tp_count,
         ep_count,
     )
+    new_state, final = update_state(state, key, value, final)
     return (final, new_state)
 
 

time: 63.3 us -> 52.4 us (0.83)
  local copies, waits for them, and re-layouts: 12.6 us -> 0 us
  Pallas kernels: 49.3 us -> 50.9 us
    unnamed x23 -> x0, local copies, waits for them, and re-layouts: 12.6 us -> none
    pallas_call x2, Pallas kernels: 49.3 us -> 50.9 us  [the longest x1 46.4 us: layer(): pl.pallas_call(functools.partial(layer_kernel, tp_count, ep_count, slots,...]
where the time goes in v3:
time: 52.4 us; the launch traced here: 51.6 us
  Pallas kernels  50.9 us (97%)
  between operations  0.65 us (1%)
    pallas_call x1, Pallas kernels, layer(): pl.pallas_call(functools.partial(layer_kernel, tp_count, ep_count, slots,...  46.4 us
    pallas_call x1, Pallas kernels, update_state(): pl.pallas_call(state_kernel, out_shape=(jax.ShapeDtypeStruct(state.shape,...  4.57 us

profile of v3, /device:TPU:0, one launch (start us, length us, event | category | flops | bytes accessed | tf_op | source)
XLA Modules:
  0.0 51.6 jit_solution(14723215773931097997)
XLA Ops:
  0.6 46.4 %layer.1 = (bf16[32,512]{1,0:T(8,128)(2,1)}, f32[2,128,32]{2,1,0:T(8,128)}, f32[32,256]{1,0:T(8,128)}) custom-call(bf16[32,2048]{1,0:T(8,128)(2,1)} %resid.1, bf16[2048]{0:T(1024)(128)(2,1)} %norm_gain.1, s32[32]{0:T(128)} %positions.1, f32[1,128]{1,0:T(1,128)} %constant.2.clone.freq, bf16[256]{0:T(256)(128)(2,1)} %head_gain.1, bf16[2048]{0:T(1024)(128)(2,1)} %ffn_gain.1, ...), custom_call_target="tpu_custom_call" | custom-call | tf_op jit(solution)/shard_map/layer/pallas_call | solution.py:588
  47.0 4.6 %update_state.1 = (f32[32,2,128,128]{3,2,1,0:T(8,128)}, bf16[32,512]{1,0:T(8,128)(2,1)}) custom-call(f32[32,2,128,128]{3,2,1,0:T(8,128)} %state.3, f32[2,128,32]{2,1,0:T(8,128)} %get-tuple-element.7.key, f32[32,256]{1,0:T(8,128)} %get-tuple-element.8.value, bf16[32,512]{1,0:T(8,128)(2,1)} %get-tuple-element.9.final), custom_call_target="tpu_custom_call" | custom-call | tf_op jit(solution)/shard_map/update_state/pallas_call | solution.py:83

commit v4 on v3

--- a/solution.py
+++ b/solution.py
@@ -194,6 +194,8 @@
     er_far,
     do_tx,
     do_rx,
+    relay_tx,
+    relay_rx,
     mo_tx,
     mo_rx,
     fetch_sem,
@@ -206,7 +208,6 @@
     me_e = lax.axis_index("ep")
     seq_dev, model_width = resid_ref.shape
     width = model_width // tp_count
-    block = hidden.shape[0] // tp_count
     f32 = jnp.float32
     bf16 = jnp.bfloat16
 
@@ -448,47 +449,102 @@
         send(inverses.at[me_e], inverses.at[me_e], (peer_e(d), me_t)) for d in ep_steps
     ]
 
+    sources = ep_count // 2
+    masks = [list(range(1, sources)), list(range(sources, ep_count))]
+    side = lax.div(me_e, sources)
+    sides = [side, 1 - side]
+    core = lax.rem(me_t, 2)
+    group_rows = sources * seq_dev
+    share = group_rows // tp_count
+    owners = share // seq_dev
+    pair_of = lax.div(me_t, 2)
+    by_mask = {d: copy for d, copy in zip(ep_steps, gathered)}
+
+    def fill_tokens(g):
+        for i in range(sources):
+            s = sides[g] * sources + i
+            tokens[me_t, span(s, slots), :] = dot(hot[s], rows[s]).astype(bf16)
+        place = span(sides[g], sources * slots)
+        return spread(lambda index: tokens.at[index, place, :])
+
+    def gate_up(g):
+        group = rows[pl.ds(sides[g] * sources, sources)].reshape(group_rows, width)
+        for which, weight in enumerate((wg, wu)):
+            if g == 0:
+                ready(1 + which)
+            product = lax.dot_general(
+                group, weight[...], (((1,), (1,)), ((), ())), preferred_element_type=f32
+            ).astype(bf16)
+            for t in range(tp_count):
+                gu_tx[g, t % 2, t // 2, which] = product[t * share : (t + 1) * share]
+        return send(gu_tx.at[g, 1 - core], gu_rx.at[g], (me_e, sibling))
+
+    def pair_up(g, near):
+        arrive([near])
+        sent = []
+        for k in range(1, half):
+            p = flip(pair_of, k)
+            gu_pair[g, k - 1] = (
+                gu_tx[g, core, p].astype(f32) + gu_rx[g, p].astype(f32)
+            ).astype(bf16)
+            sent.append(send(gu_pair.at[g, k - 1], gu_far.at[g, k - 1], (me_e, across(k))))
+        return sent
+
+    def activate(g, far):
+        arrive(far)
+        factor = jnp.concatenate(
+            [
+                to_column(inverses[sides[g] * sources + me_t * owners + i, 0:1, :])
+                for i in range(owners)
+            ],
+            axis=0,
+        )
+        total = gu_tx[g, core, pair_of].astype(f32) + gu_rx[g, pair_of].astype(f32)
+        for k in range(1, half):
+            total = total + gu_far[g, k - 1].astype(f32)
+        hidden[g, me_t] = (jax.nn.silu(total[0] * factor) * (total[1] * factor)).astype(bf16)
+        return spread(lambda index: hidden.at[g, index])
+
+    def share_hidden(g, hids):
+        return pass_on(hids, lambda index: hidden.at[g, index])
+
+    def lower(g, hids):
+        arrive(hids)
+        product = dot(hidden[g].reshape(group_rows, hidden.shape[-1]), wd[...])
+        do_tx[g] = product.astype(bf16).reshape(sources, seq_dev, width)
+        return [
+            send(
+                do_tx.at[g, lax.rem(peer_e(d), sources)],
+                do_rx.at[g, d - 1],
+                (peer_e(d), me_t),
+            )
+            for d in reversed(masks[0])
+        ]
+
+    def forward(copies, g):
+        place = span(sides[g], sources * slots)
+        return pass_on(copies, lambda index: tokens.at[index, place, :])
+
     arrive(hots)
-    arrive(gathered)
-    for s in range(ep_count):
-        tokens[me_t, s * slots : (s + 1) * slots, :] = dot(hot[s], rows[s]).astype(bf16)
-    toks = spread(lambda index: tokens.at[index])
-    near = []
-    all_rows = rows[...].reshape(ep_count * seq_dev, width)
-    for which, weight in enumerate((wg, wu)):
-        ready(1 + which)
-        gu_tx[which] = lax.dot_general(
-            all_rows, weight[...], (((1,), (1,)), ((), ())), preferred_element_type=f32
-        ).astype(bf16)
-        near.append(
-            [
-                send(
-                    gu_tx.at[which, span(flip(sibling, 2 * k), block), :],
-                    gu_rx.at[which, k],
-                    (me_e, sibling),
-                )
-                for k in range(half)
-            ]
-        )
-    toks = pass_on(toks, lambda index: tokens.at[index])
-    far = []
-    for which in range(2):
-        arrive(near[which])
-        for k in range(1, half):
-            target = across(k)
-            gu_pair[which, k - 1] = (
-                gu_tx[which, span(target, block), :].astype(f32) + gu_rx[which, k].astype(f32)
-            ).astype(bf16)
-            far.append(
-                send(gu_pair.at[which, k - 1], gu_far.at[which, k - 1], (me_e, target))
-            )
+    arrive([by_mask[d] for d in masks[0]])
+    toks = fill_tokens(0)
+    near_0 = gate_up(0)
+    far_0 = pair_up(0, near_0)
+    arrive([by_mask[d] for d in masks[1]])
+    toks_far = fill_tokens(1)
+    near_1 = gate_up(1)
+    toks = forward(toks, 0)
+    far_1 = pair_up(1, near_1)
     arrive(factors)
+    hid_0 = activate(0, far_0)
     for s in range(ep_count):
         token_scale[s * slots : (s + 1) * slots, :] = jnp.sum(
             hot[s].astype(f32) * inverses[s, 0:1, 0:seq_dev], axis=1, keepdims=True
         )
+    toks_far = forward(toks_far, 1)
+    hid_1 = activate(1, far_1)
     ready(3, 4)
-    arrive(toks)
+    arrive(toks + toks_far)
     tile = min(256, eg.shape[1])
 
     def expert_tile(index, carry):
@@ -510,21 +566,8 @@
         target = flip(sibling, 2 * k)
         er_tx[k] = dot(eh[...], ed[:, span(target, width)]).astype(bf16)
         pairs.append(send(er_tx.at[k], er_rx.at[k], (me_e, sibling)))
-    arrive(far)
-    factor = jnp.concatenate(
-        [
-            to_column(inverses[me_t * (block // seq_dev) + i, 0:1, :])
-            for i in range(block // seq_dev)
-        ],
-        axis=0,
-    )
-    gate = gu_tx[0, span(me_t, block), :].astype(f32) + gu_rx[0, 0].astype(f32)
-    up = gu_tx[1, span(me_t, block), :].astype(f32) + gu_rx[1, 0].astype(f32)
-    for k in range(1, half):
-        gate = gate + gu_far[0, k - 1].astype(f32)
-        up = up + gu_far[1, k - 1].astype(f32)
-    hidden[span(me_t, block), :] = (jax.nn.silu(gate * factor) * (up * factor)).astype(bf16)
-    hids = spread(lambda index: hidden.at[span(index, block), :])
+    hid_0 = share_hidden(0, hid_0)
+    hid_1 = share_hidden(1, hid_1)
     partials = []
     for k in range(1, half):
         target = across(k)
@@ -532,17 +575,19 @@
         arrive(pairs[k : k + 1])
         er_pair[k - 1] = (summed + er_rx[k].astype(f32)).astype(bf16)
         partials.append(send(er_pair.at[k - 1], er_far.at[k - 1], (me_e, target)))
+    ready(6)
+    outs_far = lower(1, hid_1)
+    outs = lower(0, hid_0)
     result = dot(eh[...], ed[:, own])
     arrive(pairs[:1])
     result = result + er_rx[0].astype(f32)
-    hids = pass_on(hids, lambda index: hidden.at[span(index, block), :])
-    ready(6)
-    arrive(hids)
-    do_tx[...] = dot(hidden[...], wd[...]).astype(bf16)
-    outs = [
-        send(do_tx.at[span(peer_e(d), seq_dev), :], do_rx.at[d - 1], (peer_e(d), me_t))
-        for d in ep_steps
-    ]
+    arrive(outs_far)
+    place = lax.rem(me_e, sources)
+    relayed = do_tx[1, place].astype(f32)
+    for d in masks[0]:
+        relayed = relayed + do_rx[1, d - 1].astype(f32)
+    relay_tx[...] = relayed.astype(bf16)
+    outs.append(send(relay_tx, relay_rx, (peer_e(sources), me_t)))
     arrive(partials)
     for k in range(1, half):
         result = result + er_far[k - 1].astype(f32)
@@ -554,9 +599,9 @@
     ]
     mo_rx[place, :] = mo_tx[place, :]
     arrive(outs)
-    dense = do_tx[span(me_e, seq_dev), :].astype(f32)
-    for d in ep_steps:
-        dense = dense + do_rx[d - 1].astype(f32)
+    dense = do_tx[0, lax.rem(me_e, sources)].astype(f32) + relay_rx[...].astype(f32)
+    for d in masks[0]:
+        dense = dense + do_rx[0, d - 1].astype(f32)
     partly = middle[...] + mixing * dense
     arrive(backs)
     returned = lax.dot_general(
@@ -573,7 +618,7 @@
     chunks = min(8, seq_dev)
     width = model_width // tp_count
     batch = seq_dev * ep_count
-    block = batch // tp_count
+    share = batch // 2 // tp_count
     dense_units = weights[1].shape[0]
     half = tp_count // 2
     expert_units = weights[4].shape[2]
@@ -582,7 +627,7 @@
     f32 = jnp.float32
     peers_t = tp_count - 1
     peers_e = ep_count - 1
-    copies = 7 * peers_t + 5 * peers_e
+    copies = 3 * peers_t + 5 * peers_e + 2 * (2 * (2 * half - 1) + half) + 2 * half
     vmem = pl.BlockSpec(memory_space=pltpu.VMEM)
     anywhere = pl.BlockSpec(memory_space=pltpu.HBM)
     return pl.pallas_call(
@@ -620,18 +665,20 @@
             pltpu.VMEM((ep_count, slots, seq_dev), bf16),
             pltpu.VMEM((tp_count, items, width), bf16),
             pltpu.VMEM((items, 1), f32),
-            pltpu.VMEM((2, batch, dense_units), bf16),
-            pltpu.VMEM((2, half, block, dense_units), bf16),
-            pltpu.VMEM((2, half - 1, block, dense_units), bf16),
-            pltpu.VMEM((2, half - 1, block, dense_units), bf16),
-            pltpu.VMEM((batch, dense_units), bf16),
+            pltpu.VMEM((2, 2, half, 2, share, dense_units), bf16),
+            pltpu.VMEM((2, half, 2, share, dense_units), bf16),
+            pltpu.VMEM((2, half - 1, 2, share, dense_units), bf16),
+            pltpu.VMEM((2, half - 1, 2, share, dense_units), bf16),
+            pltpu.VMEM((2, tp_count, share, dense_units), bf16),
             pltpu.VMEM((items, expert_units), bf16),
             pltpu.VMEM((half, items, width), bf16),
             pltpu.VMEM((half, items, width), bf16),
             pltpu.VMEM((half - 1, items, width), bf16),
             pltpu.VMEM((half - 1, items, width), bf16),
-            pltpu.VMEM((batch, width), bf16),
-            pltpu.VMEM((peers_e, seq_dev, width), bf16),
+            pltpu.VMEM((2, ep_count // 2, seq_dev, width), bf16),
+            pltpu.VMEM((2, ep_count // 2 - 1, seq_dev, width), bf16),
+            pltpu.VMEM((seq_dev, width), bf16),
+            pltpu.VMEM((seq_dev, width), bf16),
             pltpu.VMEM((items, width), bf16),
             pltpu.VMEM((items, width), bf16),
             pltpu.SemaphoreType.DMA((13,)),

time: 52.4 us -> 50.8 us (0.969); the launches traced: 51.6 us -> 50.6 us
  Pallas kernels: 50.9 us -> 50 us
    pallas_call x1, Pallas kernels: 46.4 us -> 45.4 us  [layer(): pl.pallas_call(functools.partial(layer_kernel, tp_count, ep_count, slots,...]
where the time goes in v4:
time: 50.8 us; the launch traced here: 50.6 us
  Pallas kernels  50 us (98%)
  between operations  0.65 us (1%)
    pallas_call x1, Pallas kernels, layer(): pl.pallas_call(functools.partial(layer_kernel, tp_count, ep_count, slots,...  45.4 us
    pallas_call x1, Pallas kernels, update_state(): pl.pallas_call(state_kernel, out_shape=(jax.ShapeDtypeStruct(state.shape,...  4.57 us

profile of v4, /device:TPU:0, one launch (start us, length us, event | category | flops | bytes accessed | tf_op | source)
XLA Modules:
  0.0 50.6 jit_solution(16752352173148533962)
XLA Ops:
  0.6 45.4 %layer.1 = (bf16[32,512]{1,0:T(8,128)(2,1)}, f32[2,128,32]{2,1,0:T(8,128)}, f32[32,256]{1,0:T(8,128)}) custom-call(bf16[32,2048]{1,0:T(8,128)(2,1)} %resid.1, bf16[2048]{0:T(1024)(128)(2,1)} %norm_gain.1, s32[32]{0:T(128)} %positions.1, f32[1,128]{1,0:T(1,128)} %constant.2.clone.freq, bf16[256]{0:T(256)(128)(2,1)} %head_gain.1, bf16[2048]{0:T(1024)(128)(2,1)} %ffn_gain.1, ...), custom_call_target="tpu_custom_call" | custom-call | tf_op jit(solution)/shard_map/layer/pallas_call | solution.py:633
  46.0 4.6 %update_state.1 = (f32[32,2,128,128]{3,2,1,0:T(8,128)}, bf16[32,512]{1,0:T(8,128)(2,1)}) custom-call(f32[32,2,128,128]{3,2,1,0:T(8,128)} %state.3, f32[2,128,32]{2,1,0:T(8,128)} %get-tuple-element.7.key, f32[32,256]{1,0:T(8,128)} %get-tuple-element.8.value, bf16[32,512]{1,0:T(8,128)(2,1)} %get-tuple-element.9.final), custom_call_target="tpu_custom_call" | custom-call | tf_op jit(solution)/shard_map/update_state/pallas_call | solution.py:83

commit v5 on v4

--- a/solution.py
+++ b/solution.py
@@ -78,7 +78,7 @@
 
 
 def update_state(state, key, value, final):
-    chunks = min(8, state.shape[0])
+    chunks = min(4, state.shape[0])
     anywhere = pl.BlockSpec(memory_space=pltpu.HBM)
     return pl.pallas_call(
         state_kernel,
@@ -254,7 +254,7 @@
             )
         )
     ]
-    for copy in fetches + states + loads[:1]:
+    for copy in fetches:
         copy.start()
 
     def ready(*indices):
@@ -316,8 +316,11 @@
     half = tp_count // 2
     sibling = peer_t(1)
 
+    def cross(step):
+        return 2 * step + step.bit_count() % 2
+
     def across(step):
-        return peer_t(2 * step)
+        return peer_t(cross(step))
 
     def spread(at):
         return [
@@ -335,6 +338,8 @@
     own = span(me_t, width)
     for copy in fetches[:5]:
         copy.wait()
+    for copy in states + loads[:1]:
+        copy.start()
     normed = rms_norm(resid_ref[...].astype(f32), norm_ref[...].reshape(1, -1)).astype(bf16)
     places = jnp.broadcast_to(place_ref[...].astype(f32).reshape(1, seqs), (size, seqs)).T
     angles = places * freq_ref[...]
@@ -423,7 +428,10 @@
     mid = resid_ref[:, own].astype(f32) + total
     scaled = mid * gain
     rows[me_e] = scaled.astype(bf16)
-    gathered = [send(rows.at[me_e], rows.at[me_e], (peer_e(d), me_t)) for d in ep_steps]
+    sources = ep_count // 2
+    near_steps = list(range(sources - 1, 0, -1))
+    mirrored = send(rows.at[me_e], rows.at[me_e], (peer_e(sources), me_t))
+    gathered = [send(rows.at[me_e], rows.at[me_e], (peer_e(d), me_t)) for d in near_steps]
     middle[...] = mid
 
     lane = lax.broadcasted_iota(jnp.int32, (seq_dev, 128), 1)
@@ -449,16 +457,13 @@
         send(inverses.at[me_e], inverses.at[me_e], (peer_e(d), me_t)) for d in ep_steps
     ]
 
-    sources = ep_count // 2
-    masks = [list(range(1, sources)), list(range(sources, ep_count))]
     side = lax.div(me_e, sources)
     sides = [side, 1 - side]
-    core = lax.rem(me_t, 2)
+    core = lax.rem(sum(lax.div(me_t, 1 << bit) for bit in range(tp_count.bit_length() - 1)), 2)
     group_rows = sources * seq_dev
     share = group_rows // tp_count
     owners = share // seq_dev
     pair_of = lax.div(me_t, 2)
-    by_mask = {d: copy for d, copy in zip(ep_steps, gathered)}
 
     def fill_tokens(g):
         for i in range(sources):
@@ -476,7 +481,7 @@
                 group, weight[...], (((1,), (1,)), ((), ())), preferred_element_type=f32
             ).astype(bf16)
             for t in range(tp_count):
-                gu_tx[g, t % 2, t // 2, which] = product[t * share : (t + 1) * share]
+                gu_tx[g, t.bit_count() % 2, t // 2, which] = product[t * share : (t + 1) * share]
         return send(gu_tx.at[g, 1 - core], gu_rx.at[g], (me_e, sibling))
 
     def pair_up(g, near):
@@ -518,19 +523,22 @@
                 do_rx.at[g, d - 1],
                 (peer_e(d), me_t),
             )
-            for d in reversed(masks[0])
+            for d in near_steps
         ]
 
     def forward(copies, g):
         place = span(sides[g], sources * slots)
         return pass_on(copies, lambda index: tokens.at[index, place, :])
 
+    arrive([mirrored])
+    mirror = peer_e(sources)
+    passed = [send(rows.at[mirror], rows.at[mirror], (peer_e(d), me_t)) for d in near_steps]
     arrive(hots)
-    arrive([by_mask[d] for d in masks[0]])
+    arrive(gathered)
     toks = fill_tokens(0)
     near_0 = gate_up(0)
     far_0 = pair_up(0, near_0)
-    arrive([by_mask[d] for d in masks[1]])
+    arrive(passed)
     toks_far = fill_tokens(1)
     near_1 = gate_up(1)
     toks = forward(toks, 0)
@@ -560,13 +568,15 @@
         return carry
 
     lax.fori_loop(0, eg.shape[1] // tile, expert_tile, 0)
+    hid_0 = share_hidden(0, hid_0)
     ready(5)
     pairs = []
     for k in range(half):
-        target = flip(sibling, 2 * k)
+        target = flip(sibling, cross(k))
         er_tx[k] = dot(eh[...], ed[:, span(target, width)]).astype(bf16)
         pairs.append(send(er_tx.at[k], er_rx.at[k], (me_e, sibling)))
-    hid_0 = share_hidden(0, hid_0)
+    ready(6)
+    outs = lower(0, hid_0)
     hid_1 = share_hidden(1, hid_1)
     partials = []
     for k in range(1, half):
@@ -575,19 +585,10 @@
         arrive(pairs[k : k + 1])
         er_pair[k - 1] = (summed + er_rx[k].astype(f32)).astype(bf16)
         partials.append(send(er_pair.at[k - 1], er_far.at[k - 1], (me_e, target)))
-    ready(6)
     outs_far = lower(1, hid_1)
-    outs = lower(0, hid_0)
     result = dot(eh[...], ed[:, own])
     arrive(pairs[:1])
     result = result + er_rx[0].astype(f32)
-    arrive(outs_far)
-    place = lax.rem(me_e, sources)
-    relayed = do_tx[1, place].astype(f32)
-    for d in masks[0]:
-        relayed = relayed + do_rx[1, d - 1].astype(f32)
-    relay_tx[...] = relayed.astype(bf16)
-    outs.append(send(relay_tx, relay_rx, (peer_e(sources), me_t)))
     arrive(partials)
     for k in range(1, half):
         result = result + er_far[k - 1].astype(f32)
@@ -598,9 +599,15 @@
         for d in ep_steps
     ]
     mo_rx[place, :] = mo_tx[place, :]
+    arrive(outs_far)
+    relayed = do_tx[1, lax.rem(me_e, sources)].astype(f32)
+    for d in near_steps:
+        relayed = relayed + do_rx[1, d - 1].astype(f32)
+    relay_tx[...] = relayed.astype(bf16)
+    outs.append(send(relay_tx, relay_rx, (peer_e(sources), me_t)))
     arrive(outs)
     dense = do_tx[0, lax.rem(me_e, sources)].astype(f32) + relay_rx[...].astype(f32)
-    for d in masks[0]:
+    for d in near_steps:
         dense = dense + do_rx[0, d - 1].astype(f32)
     partly = middle[...] + mixing * dense
     arrive(backs)
@@ -615,7 +622,7 @@
 def layer(smalls, slots, projections, state, weights, tp_count, ep_count):
     seq_dev, model_width = smalls[0].shape
     _, heads, size, _ = state.shape
-    chunks = min(8, seq_dev)
+    chunks = min(4, seq_dev)
     width = model_width // tp_count
     batch = seq_dev * ep_count
     share = batch // 2 // tp_count

time: 50.8 us -> 48.8 us (0.961)
  Pallas kernels: 50 us -> 48.1 us
    pallas_call x1, Pallas kernels: 45.4 us -> 43.8 us  [layer(): pl.pallas_call(functools.partial(layer_kernel, tp_count, ep_count, slots,...]
where the time goes in v5:
time: 48.8 us; the launch traced here: 48.7 us
  Pallas kernels  48.1 us (99%)
  between operations  0.65 us (1%)
    pallas_call x1, Pallas kernels, layer(): pl.pallas_call(functools.partial(layer_kernel, tp_count, ep_count, slots,...  43.8 us
    pallas_call x1, Pallas kernels, update_state(): pl.pallas_call(state_kernel, out_shape=(jax.ShapeDtypeStruct(state.shape,...  4.24 us

profile of v5, /device:TPU:0, one launch (start us, length us, event | category | flops | bytes accessed | tf_op | source)
XLA Modules:
  0.0 48.7 jit_solution(15506324494916283120)
XLA Ops:
  0.6 43.8 %layer.1 = (bf16[32,512]{1,0:T(8,128)(2,1)}, f32[2,128,32]{2,1,0:T(8,128)}, f32[32,256]{1,0:T(8,128)}) custom-call(bf16[32,2048]{1,0:T(8,128)(2,1)} %resid.1, bf16[2048]{0:T(1024)(128)(2,1)} %norm_gain.1, s32[32]{0:T(128)} %positions.1, f32[1,128]{1,0:T(1,128)} %constant.2.clone.freq, bf16[256]{0:T(256)(128)(2,1)} %head_gain.1, bf16[2048]{0:T(1024)(128)(2,1)} %ffn_gain.1, ...), custom_call_target="tpu_custom_call" | custom-call | tf_op jit(solution)/shard_map/layer/pallas_call | solution.py:640
  44.5 4.2 %update_state.1 = (f32[32,2,128,128]{3,2,1,0:T(8,128)}, bf16[32,512]{1,0:T(8,128)(2,1)}) custom-call(f32[32,2,128,128]{3,2,1,0:T(8,128)} %state.3, f32[2,128,32]{2,1,0:T(8,128)} %get-tuple-element.7.key, f32[32,256]{1,0:T(8,128)} %get-tuple-element.8.value, bf16[32,512]{1,0:T(8,128)(2,1)} %get-tuple-element.9.final), custom_call_target="tpu_custom_call" | custom-call | tf_op jit(solution)/shard_map/update_state/pallas_call | solution.py:83

commit v6 on v5

--- a/solution.py
+++ b/solution.py
@@ -589,6 +589,12 @@
     result = dot(eh[...], ed[:, own])
     arrive(pairs[:1])
     result = result + er_rx[0].astype(f32)
+    arrive(outs_far)
+    relayed = do_tx[1, lax.rem(me_e, sources)].astype(f32)
+    for d in near_steps:
+        relayed = relayed + do_rx[1, d - 1].astype(f32)
+    relay_tx[...] = relayed.astype(bf16)
+    outs.append(send(relay_tx, relay_rx, (peer_e(sources), me_t)))
     arrive(partials)
     for k in range(1, half):
         result = result + er_far[k - 1].astype(f32)
@@ -599,12 +605,6 @@
         for d in ep_steps
     ]
     mo_rx[place, :] = mo_tx[place, :]
-    arrive(outs_far)
-    relayed = do_tx[1, lax.rem(me_e, sources)].astype(f32)
-    for d in near_steps:
-        relayed = relayed + do_rx[1, d - 1].astype(f32)
-    relay_tx[...] = relayed.astype(bf16)
-    outs.append(send(relay_tx, relay_rx, (peer_e(sources), me_t)))
     arrive(outs)
     dense = do_tx[0, lax.rem(me_e, sources)].astype(f32) + relay_rx[...].astype(f32)
     for d in near_steps:
@@ -622,7 +622,7 @@
 def layer(smalls, slots, projections, state, weights, tp_count, ep_count):
     seq_dev, model_width = smalls[0].shape
     _, heads, size, _ = state.shape
-    chunks = min(4, seq_dev)
+    chunks = min(2, seq_dev)
     width = model_width // tp_count
     batch = seq_dev * ep_count
     share = batch // 2 // tp_count

time: 48.8 us -> 48 us (0.984)
  Pallas kernels: 48.1 us -> 47.2 us
    pallas_call x1, Pallas kernels: 43.8 us -> 43 us  [layer(): pl.pallas_call(functools.partial(layer_kernel, tp_count, ep_count, slots,...]
where the time goes in v6:
time: 48 us; the launch traced here: 47.9 us
  Pallas kernels  47.2 us (98%)
  between operations  0.65 us (1%)
    pallas_call x1, Pallas kernels, layer(): pl.pallas_call(functools.partial(layer_kernel, tp_count, ep_count, slots,...  43 us
    pallas_call x1, Pallas kernels, update_state(): pl.pallas_call(state_kernel, out_shape=(jax.ShapeDtypeStruct(state.shape,...  4.24 us

profile of v6, /device:TPU:0, one launch (start us, length us, event | category | flops | bytes accessed | tf_op | source)
XLA Modules:
  0.0 47.9 jit_solution(4861202797988887753)
XLA Ops:
  0.6 43.0 %layer.1 = (bf16[32,512]{1,0:T(8,128)(2,1)}, f32[2,128,32]{2,1,0:T(8,128)}, f32[32,256]{1,0:T(8,128)}) custom-call(bf16[32,2048]{1,0:T(8,128)(2,1)} %resid.1, bf16[2048]{0:T(1024)(128)(2,1)} %norm_gain.1, s32[32]{0:T(128)} %positions.1, f32[1,128]{1,0:T(1,128)} %constant.2.clone.freq, bf16[256]{0:T(256)(128)(2,1)} %head_gain.1, bf16[2048]{0:T(1024)(128)(2,1)} %ffn_gain.1, ...), custom_call_target="tpu_custom_call" | custom-call | tf_op jit(solution)/shard_map/layer/pallas_call | solution.py:640
  43.6 4.2 %update_state.1 = (f32[32,2,128,128]{3,2,1,0:T(8,128)}, bf16[32,512]{1,0:T(8,128)(2,1)}) custom-call(f32[32,2,128,128]{3,2,1,0:T(8,128)} %state.3, f32[2,128,32]{2,1,0:T(8,128)} %get-tuple-element.7.key, f32[32,256]{1,0:T(8,128)} %get-tuple-element.8.value, bf16[32,512]{1,0:T(8,128)(2,1)} %get-tuple-element.9.final), custom_call_target="tpu_custom_call" | custom-call | tf_op jit(solution)/shard_map/update_state/pallas_call | solution.py:83

commit v7 on v6

--- a/solution.py
+++ b/solution.py
@@ -196,6 +196,7 @@
     do_rx,
     relay_tx,
     relay_rx,
+    own_sum,
     mo_tx,
     mo_rx,
     fetch_sem,
@@ -578,32 +579,42 @@
     ready(6)
     outs = lower(0, hid_0)
     hid_1 = share_hidden(1, hid_1)
-    partials = []
+    partials = [[], []]
+    slot_places = [span(sides[g], sources * slots) for g in range(2)]
     for k in range(1, half):
         target = across(k)
         summed = dot(eh[...], ed[:, span(target, width)])
         arrive(pairs[k : k + 1])
         er_pair[k - 1] = (summed + er_rx[k].astype(f32)).astype(bf16)
-        partials.append(send(er_pair.at[k - 1], er_far.at[k - 1], (me_e, target)))
+        for g in (1, 0):
+            at = slot_places[g]
+            partials[g].append(
+                send(er_pair.at[k - 1, at], er_far.at[k - 1, at], (me_e, target))
+            )
     outs_far = lower(1, hid_1)
     result = dot(eh[...], ed[:, own])
     arrive(pairs[:1])
-    result = result + er_rx[0].astype(f32)
+    own_sum[...] = result + er_rx[0].astype(f32)
     arrive(outs_far)
     relayed = do_tx[1, lax.rem(me_e, sources)].astype(f32)
     for d in near_steps:
         relayed = relayed + do_rx[1, d - 1].astype(f32)
     relay_tx[...] = relayed.astype(bf16)
     outs.append(send(relay_tx, relay_rx, (peer_e(sources), me_t)))
-    arrive(partials)
-    for k in range(1, half):
-        result = result + er_far[k - 1].astype(f32)
-    mo_tx[...] = result.astype(bf16)
     place = span(me_e, slots)
-    backs = [
-        send(mo_tx.at[span(peer_e(d), slots), :], mo_rx.at[place, :], (peer_e(d), me_t))
-        for d in ep_steps
-    ]
+    backs = []
+    for g in (1, 0):
+        arrive(partials[g])
+        at = slot_places[g]
+        result = own_sum[at, :]
+        for k in range(1, half):
+            result = result + er_far[k - 1, at].astype(f32)
+        mo_tx[at, :] = result.astype(bf16)
+        steps = near_steps if g == 0 else list(range(ep_count - 1, sources - 1, -1))
+        backs += [
+            send(mo_tx.at[span(peer_e(d), slots), :], mo_rx.at[place, :], (peer_e(d), me_t))
+            for d in steps
+        ]
     mo_rx[place, :] = mo_tx[place, :]
     arrive(outs)
     dense = do_tx[0, lax.rem(me_e, sources)].astype(f32) + relay_rx[...].astype(f32)
@@ -634,7 +645,7 @@
     f32 = jnp.float32
     peers_t = tp_count - 1
     peers_e = ep_count - 1
-    copies = 3 * peers_t + 5 * peers_e + 2 * (2 * (2 * half - 1) + half) + 2 * half
+    copies = 3 * peers_t + 5 * peers_e + 2 * (2 * (2 * half - 1) + half) + 3 * half
     vmem = pl.BlockSpec(memory_space=pltpu.VMEM)
     anywhere = pl.BlockSpec(memory_space=pltpu.HBM)
     return pl.pallas_call(
@@ -686,6 +697,7 @@
             pltpu.VMEM((2, ep_count // 2 - 1, seq_dev, width), bf16),
             pltpu.VMEM((seq_dev, width), bf16),
             pltpu.VMEM((seq_dev, width), bf16),
+            pltpu.VMEM((items, width), f32),
             pltpu.VMEM((items, width), bf16),
             pltpu.VMEM((items, width), bf16),
             pltpu.SemaphoreType.DMA((13,)),

time: 48 us -> 47.8 us (level)
  no operation moved by 1% of the time
where the time goes in v7:
time: 47.8 us; the launch traced here: 47.6 us
  Pallas kernels  47 us (98%)
  between operations  0.65 us (1%)
    pallas_call x1, Pallas kernels, layer(): pl.pallas_call(functools.partial(layer_kernel, tp_count, ep_count, slots,...  42.7 us
    pallas_call x1, Pallas kernels, update_state(): pl.pallas_call(state_kernel, out_shape=(jax.ShapeDtypeStruct(state.shape,...  4.24 us

profile of v7, /device:TPU:0, one launch (start us, length us, event | category | flops | bytes accessed | tf_op | source)
XLA Modules:
  0.0 47.6 jit_solution(17713455890278260545)
XLA Ops:
  0.6 42.7 %layer.1 = (bf16[32,512]{1,0:T(8,128)(2,1)}, f32[2,128,32]{2,1,0:T(8,128)}, f32[32,256]{1,0:T(8,128)}) custom-call(bf16[32,2048]{1,0:T(8,128)(2,1)} %resid.1, bf16[2048]{0:T(1024)(128)(2,1)} %norm_gain.1, s32[32]{0:T(128)} %positions.1, f32[1,128]{1,0:T(1,128)} %constant.2.clone.freq, bf16[256]{0:T(256)(128)(2,1)} %head_gain.1, bf16[2048]{0:T(1024)(128)(2,1)} %ffn_gain.1, ...), custom_call_target="tpu_custom_call" | custom-call | tf_op jit(solution)/shard_map/layer/pallas_call | solution.py:651
  43.4 4.2 %update_state.1 = (f32[32,2,128,128]{3,2,1,0:T(8,128)}, bf16[32,512]{1,0:T(8,128)(2,1)}) custom-call(f32[32,2,128,128]{3,2,1,0:T(8,128)} %state.3, f32[2,128,32]{2,1,0:T(8,128)} %get-tuple-element.7.key, f32[32,256]{1,0:T(8,128)} %get-tuple-element.8.value, bf16[32,512]{1,0:T(8,128)(2,1)} %get-tuple-element.9.final), custom_call_target="tpu_custom_call" | custom-call | tf_op jit(solution)/shard_map/update_state/pallas_call | solution.py:83
